TPU v7x, 256 devices: a whole 4x4x8 slice. The times are simulated.
256 devices in a mesh: ep: 64 (over z, y, core), tp: 4 (over x).
Axes of the slice: x: 4, y: 4, z: 8, core: 2. Of those that a mesh axis runs over, the one named last changes fastest.
Arguments:
- tokens: bfloat16 [512, 2048], P('ep'), may hold values from -4 to 4
- w_query: bfloat16 [2048, 1024], P(None, 'tp'), may hold values from -0.125 to 0.125
- w_key: bfloat16 [2048, 1024], P(None, 'tp'), may hold values from -0.125 to 0.125
- w_value: bfloat16 [2048, 1024], P(None, 'tp'), may hold values from -0.125 to 0.125
- w_outgate: bfloat16 [2048, 1024], P(None, 'tp'), may hold values from -0.125 to 0.125
- w_igate: bfloat16 [2048, 4], P(None, 'tp'), may hold values from -0.125 to 0.125
- w_fgate: bfloat16 [2048, 4], P(None, 'tp'), may hold values from -0.125 to 0.125
- forget_bias: float32 [4], P('tp'), may hold values from -1 to 5
- w_out: bfloat16 [1024, 2048], P('tp'), may hold values from -0.1875 to 0.1875
- gain_mix: float32 [2048], replicated, may hold values from 0.1 to 1.9
- gain_moe: float32 [2048], replicated, may hold values from 0.1 to 1.9
- memory: float32 [512, 4, 256, 256], P('ep', 'tp'), may hold values from -0.4 to 0.4
- normalizer: float32 [512, 4, 256], P('ep', 'tp'), may hold values from -0.8 to 0.8
- stabilizer: float32 [512, 4], P('ep', 'tp'), may hold values from 0 to 2
- expert_gate: bfloat16 [64, 2048, 512], P('ep', None, 'tp'), may hold values from -0.125 to 0.125
- expert_up: bfloat16 [64, 2048, 512], P('ep', None, 'tp'), may hold values from -0.125 to 0.125
- expert_down: bfloat16 [64, 512, 2048], P('ep', 'tp'), may hold values from -1 to 1
- routes: int32 [512, 4], P('ep'), may hold values from 0 to 63, all different within a row; in each aligned block of 8 rows (0 to 7, 8 to 15, ...) at most 2 rows name the same one
- route_weight: float32 [512, 4], P('ep'), may hold values from 0.2 to 1
Outputs:
- output: bfloat16 [512, 2048], P('ep', 'tp')
- memory_next: float32 [512, 4, 256, 256], P('ep', 'tp')
- norm_next: float32 [512, 4, 256], P('ep', 'tp')
- stabilizer_next: float32 [512, 4], P('ep', 'tp')
Inputs may be any that keep to these rules, and one draw needn't show every extreme that they name: `routes`: each row names 4 different experts. Among the 8 rows of one device (aligned blocks), no expert is named more than 2 times, a bound that some block reaches.
All inputs are finite; a program needn't handle non-finite values.
Results may differ from a plain program's by a relative error of at most 0.029.
Values may be sent and summed in bfloat16 or wider, within the bound.
A program may use at most 64 MiB of HBM per device.

v0:
```python
import math

import jax
import jax.numpy as jnp
from jax import lax
from jax.sharding import PartitionSpec as P


def copy_for_each(value, axis):
    size = lax.axis_size(axis)
    return lax.all_to_all(
        jnp.broadcast_to(value[None], (size, *value.shape)), axis, 0, 0, tiled=True
    )


def over_copies(value, axis):
    everything = copy_for_each(value, axis)
    return jnp.sum(everything.astype(jnp.float32), axis=0)


def cut_along(value, dim, size):
    before, after = (value.shape[:dim], value.shape[dim + 1 :])
    return jnp.moveaxis(value.reshape(*before, size, -1, *after), dim, 0)


def sent_and_summed(value, axis, dim):
    size = lax.axis_size(axis)
    parts = lax.all_to_all(cut_along(value, dim, size), axis, 0, 0, tiled=True)
    return jnp.sum(parts, axis=0)


def layer_norm(row_data, gain_vec):
    values = row_data.astype(jnp.float32)
    row_mean = jnp.mean(values, -1, keepdims=True)
    centered = values - row_mean
    variance = jnp.mean(centered * centered, -1, keepdims=True)
    return centered * lax.rsqrt(variance + 1e-05) * gain_vec


def slot_targets(routes, experts, capacity):
    flat_routes = routes.reshape(-1)
    onehot = (flat_routes[:, None] == jnp.arange(experts, dtype=jnp.int32)[None, :]).astype(
        jnp.int32
    )
    before = jnp.cumsum(onehot, axis=0) - onehot
    slot_index = jnp.sum(before * onehot, axis=1)
    return flat_routes * capacity + slot_index


def shards(
    tokens,
    w_query,
    w_key,
    w_value,
    w_outgate,
    w_igate,
    w_fgate,
    forget_bias,
    w_out,
    gain_mix,
    gain_moe,
    memory,
    normalizer,
    stabilizer,
    expert_gate,
    expert_up,
    expert_down,
    routes,
    route_weight,
):
    seq_rows = tokens.shape[0]
    model_width = tokens.shape[1]
    head_count = memory.shape[1]
    head_size = memory.shape[2]
    head_cols = head_count * head_size
    normed = layer_norm(tokens, gain_mix).astype(jnp.bfloat16)
    gate_in = jnp.dot(normed, w_igate, preferred_element_type=jnp.float32)
    gate_forget = jnp.dot(normed, w_fgate, preferred_element_type=jnp.float32)
    weights = (w_query, w_key, w_value, w_outgate)
    projected = jnp.concatenate(
        [jnp.dot(normed, weight, preferred_element_type=jnp.float32) for weight in weights], axis=1
    )
    rounded = projected.astype(jnp.bfloat16).reshape(seq_rows, 4, head_count, head_size)
    queries = rounded[:, 0].astype(jnp.float32)
    keys_scaled = rounded[:, 1].astype(jnp.float32) / math.sqrt(head_size)
    values_rows = rounded[:, 2].astype(jnp.float32)
    out_gate = rounded[:, 3].astype(jnp.float32)
    log_forget = jax.nn.log_sigmoid(gate_forget + forget_bias)
    stabilizer_next = jnp.maximum(log_forget + stabilizer, gate_in)
    keep_rate = jnp.exp(log_forget + stabilizer - stabilizer_next)
    admit_rate = jnp.exp(gate_in - stabilizer_next)
    memory_next = (
        keep_rate[:, :, None, None] * memory
        + admit_rate[:, :, None, None] * keys_scaled[:, :, :, None] * values_rows[:, :, None, :]
    )
    norm_next = keep_rate[:, :, None] * normalizer + admit_rate[:, :, None] * keys_scaled
    numerator = jnp.einsum("shk,shkv->shv", queries, memory_next, precision=lax.Precision.HIGHEST)
    denominator = jnp.sum(queries * norm_next, axis=-1)
    readout = numerator / jnp.maximum(jnp.abs(denominator), jnp.exp(-stabilizer_next))[:, :, None]
    mixed = (jax.nn.sigmoid(out_gate) * readout).astype(jnp.bfloat16).reshape(seq_rows, head_cols)
    head_part = jnp.dot(mixed, w_out, preferred_element_type=jnp.float32).astype(jnp.bfloat16)
    summed = over_copies(head_part, "tp").astype(jnp.float32)
    residual = tokens.astype(jnp.float32) + summed
    expert_in = layer_norm(residual, gain_moe).astype(jnp.bfloat16)
    top_count = routes.shape[1]
    local_experts = expert_gate.shape[0]
    expert_count = local_experts * lax.axis_size("ep")
    capacity = max(2, 2 * seq_rows * top_count // expert_count)
    target = slot_targets(routes, expert_count, capacity)
    outbound = (
        jnp.zeros((expert_count * capacity, model_width), jnp.bfloat16)
        .at[target]
        .set(jnp.repeat(expert_in, top_count, axis=0))
    )
    outbound = outbound.reshape(expert_count, capacity, model_width)
    quarter = model_width // lax.axis_size("tp")
    arrived = lax.all_to_all(outbound, "ep", split_axis=0, concat_axis=0, tiled=True)
    slot_count = arrived.shape[1]
    grouped = arrived.reshape(-1, local_experts, slot_count, model_width)
    gate_part = jnp.einsum(
        "aecd,edf->aecf", grouped, expert_gate, preferred_element_type=jnp.float32
    )
    up_part = jnp.einsum("aecd,edf->aecf", grouped, expert_up, preferred_element_type=jnp.float32)
    hidden = (jax.nn.silu(gate_part) * up_part).astype(jnp.bfloat16)
    partial_value, slot_count = (
        jnp.einsum("aecf,efd->aecd", hidden, expert_down, preferred_element_type=jnp.float32),
        slot_count,
    )
    reduced = sent_and_summed(partial_value, "tp", 3).astype(jnp.bfloat16)
    reduced = reduced.reshape(-1, slot_count, reduced.shape[3])
    returned = lax.all_to_all(reduced, "ep", split_axis=0, concat_axis=0, tiled=True)
    picked = jnp.take(returned.reshape(expert_count * capacity, quarter), target, axis=0).reshape(
        seq_rows, top_count, quarter
    )
    combined = jnp.sum(route_weight[:, :, None] * picked.astype(jnp.float32), axis=1)
    own_cols = lax.dynamic_slice_in_dim(residual, lax.axis_index("tp") * quarter, quarter, 1)
    output = (own_cols + combined).astype(jnp.bfloat16)
    return (output, memory_next, norm_next, stabilizer_next)


def solution(mesh):
    return jax.shard_map(
        shards,
        mesh=mesh,
        in_specs=(
            P("ep", None),
            P(None, "tp"),
            P(None, "tp"),
            P(None, "tp"),
            P(None, "tp"),
            P(None, "tp"),
            P(None, "tp"),
            P("tp"),
            P("tp", None),
            P(),
            P(),
            P("ep", "tp", None, None),
            P("ep", "tp", None),
            P("ep", "tp"),
            P("ep", None, "tp"),
            P("ep", None, "tp"),
            P("ep", "tp", None),
            P("ep", None),
            P("ep", None),
        ),
        out_specs=(P("ep", "tp"), P("ep", "tp", None, None), P("ep", "tp", None), P("ep", "tp")),
        check_vma=False,
    )
```

profile of v0, /device:TPU:1, one launch (start us, length us, event | category | flops | bytes accessed | tf_op | source)
XLA Modules:
  0.0 95.2 jit_solution(12949295463626573456)
XLA Ops:
  0.7 1.0 %convert_reduce_fusion.1 = f32[8]{0:T(128)S(1)} fusion(bf16[8,2048]{1,0:T(8,128)(2,1)} %param.19), kind=kLoop, calls=%fused_computation.40 | loop fusion | flops 32760 | bytes 32800 | tf_op jit(solution)/shard_map/reduce_sum | solution.py:34
  1.7 1.0 %fusion.28 = f32[8]{0:T(128)S(1)} fusion(bf16[8,2048]{1,0:T(8,128)(2,1)} %param.19, f32[8]{0:T(128)S(1)} %broadcast_multiply_fusion.3), kind=kLoop, calls=%fused_computation.43 | loop fusion | flops 65528 | bytes 32832 | tf_op jit(solution)/shard_map/reduce_sum | solution.py:36
  3.4 0.8 fusion.30
  4.3 0.8 convolution_bitcast_fusion.2
  5.1 0.8 exponential_bitcast_fusion
  6.0 1.5 %fusion.5 = f32[8,256]{1,0:T(8,128)S(1)} fusion(bf16[8,2048]{1,0:T(8,128)(2,1)S(1)} %fusion.30, bf16[2048,256]{1,0:T(8,128)(2,1)} %param.22), kind=kOutput, calls=%fused_computation.12 | convolution fusion | flops 8392704 | bytes 1089536 | tf_op jit(solution)/shard_map/dot_general | solution.py:81
  7.4 1.4 %broadcast_multiply_fusion = (f32[8,256]{1,0:T(8,128)S(1)}, f32[8,256]{1,0:T(8,128)S(1)}) fusion(f32[8]{0:T(128)S(1)} %multiply_bitcast_fusion, bf16[8,2048]{1,0:T(8,128)(2,1)S(1)} %fusion.30, bf16[2048,256]{1,0:T(8,128)(2,1)} %param.21), kind=kOutput, calls=%fused_computation.71 | convolution fusion | flops 8394752 | bytes 1097760 | tf_op jit(solution)/shard_map/dot_general | solution.py:81
  8.9 0.4 fusion.38
  9.3 0.5 multiply_add_fusion
  9.8 0.8 fusion
  10.7 2.0 %convolution_convert_fusion = bf16[8,2048]{1,0:T(8,128)(2,1)S(1)} fusion(bf16[256,2048]{1,0:T(8,128)(2,1)S(1)} %copy-done, bf16[8,2048]{1,0:T(8,128)(2,1)S(1)} %fusion.30, bf16[2048,256]{1,0:T(8,128)(2,1)} %param.23, f32[8,1,256]{2,1,0:T(1,128)S(1)} %fusion, f32[8]{0:T(128)S(1)} %fusion.46), kind=kOutput, calls=%fused_computation.2 | convolution fusion | flops 16809984 | bytes 2170912 | tf_op jit(solution)/shard_map/dot_general | solution.py:101
  12.6 0.7 broadcast_in_dim.13
  13.3 4.8 %all-to-all-start = ((bf16[4,8,2048]{2,1,0:T(8,128)(2,1)}), bf16[4,8,2048]{2,1,0:T(8,128)(2,1)S(1)}, u32[]{:S(2)}, u32[]{:S(2)}) async-start(bf16[4,8,2048]{2,1,0:T(8,128)(2,1)} %broadcast_in_dim.13), calls=%async_computation | async-start | bytes 262144 | tf_op jit(solution)/shard_map/all_to_all | solution.py:11
  18.7 4.3 %all-to-all-done = bf16[4,8,2048]{2,1,0:T(8,128)(2,1)S(1)} async-done(((bf16[4,8,2048]{2,1,0:T(8,128)(2,1)}), bf16[4,8,2048]{2,1,0:T(8,128)(2,1)S(1)}, u32[]{:S(2)}, u32[]{:S(2)}) %all-to-all-start) | async-done | bytes 131104 | tf_op jit(solution)/shard_map/all_to_all | solution.py:11
  23.5 1.0 %scatter_custom_fusion = bf16[128,2048]{1,0:T(8,128)(2,1)S(1)} fusion(s32[32]{0:T(128)S(1)} %fusion.45, bf16[32,2048]{1,0:T(8,128)(2,1)S(1)} %reshape.376, bf16[]{:T(256)} %constant.53.clone.1), kind=kCustom, calls=%fused_computation.35 | custom fusion | bytes 524290 | tf_op jit(solution)/shard_map/scatter | solution.py:113
  24.8 31.2 %all_to_all.20 = bf16[64,2,2048]{2,1,0:T(2,128)(2,1)S(1)} all-to-all(bf16[64,2,2048]{2,1,0:T(2,128)(2,1)S(1)} %reshape.348), channel_id=1, replica_groups=mesh['ep'=64,'tp'=4] {'ep'}, dimensions={0} | all-to-all | bytes 1048576 | tf_op jit(solution)/shard_map/all_to_all | solution.py:117
  56.4 1.8 %fusion.16 = f32[64,2,2048]{2,0,1:T(8,128)S(1)} fusion(bf16[1,128,2048]{2,1,0:T(8,128)(2,1)} %param.35, bf16[1,2048,128]{2,1,0:T(8,128)(2,1)} %param.34, bf16[64,2,2048]{2,1,0:T(2,128)(2,1)S(1)} %all_to_all.20, f32[64,1,2,128]{3,0,2,1:T(8,128)S(1)} %convolution_bitcast_fusion.1), kind=kOutput, calls=%fused_computation.29 | convolution fusion | flops 134316032 | bytes 2686976 | tf_op jit(solution)/shard_map/aecf,efd->aecd/dot_general | solution.py:126
  58.3 17.2 %all_to_all.21 = f32[4,64,1,2,512]{4,1,3,2,0:T(8,128)S(1)} all-to-all(f32[4,64,1,2,512]{4,1,3,2,0:T(8,128)S(1)} %bitcast.114), channel_id=1, replica_groups=mesh['ep'=64,'tp'=4] {'tp'}, dimensions={0} | all-to-all | bytes 2097152 | tf_op jit(solution)/shard_map/all_to_all | solution.py:28
  75.6 0.8 copy.62
  76.4 6.2 %all-to-all-start.3 = ((bf16[64,2,512]{2,1,0:T(2,128)(2,1)}), bf16[64,2,512]{2,1,0:T(2,128)(2,1)S(1)}, u32[]{:S(2)}, u32[]{:S(2)}) async-start(bf16[64,2,512]{2,1,0:T(2,128)(2,1)} %copy.62), calls=%async_computation.3 | async-start | bytes 262144 | tf_op jit(solution)/shard_map/all_to_all | solution.py:131
  82.8 0.6 copy.63
  83.4 10.3 %all-to-all-done.3 = bf16[64,2,512]{2,1,0:T(2,128)(2,1)S(1)} async-done(((bf16[64,2,512]{2,1,0:T(2,128)(2,1)}), bf16[64,2,512]{2,1,0:T(2,128)(2,1)S(1)}, u32[]{:S(2)}, u32[]{:S(2)}) %all-to-all-start.3) | async-done | bytes 131104 | tf_op jit(solution)/shard_map/all_to_all | solution.py:131
  93.8 0.6 gather_fusion
  94.5 0.6 add_convert_fusion
  (53 shorter events, 2.4 us)
Async XLA Ops:
  0.6 10.0 %copy-start = (bf16[256,2048]{1,0:T(8,128)(2,1)S(1)}, bf16[256,2048]{1,0:T(8,128)(2,1)}, u32[]{:S(2)}) copy-start(bf16[256,2048]{1,0:T(8,128)(2,1)} %param.27) | copy-start | bytes 3145732
  0.6 8.2 %copy-start.3 = (bf16[2048,256]{1,0:T(8,128)(2,1)S(1)}, bf16[2048,256]{1,0:T(8,128)(2,1)}, u32[]{:S(2)}) copy-start(bf16[2048,256]{1,0:T(8,128)(2,1)} %param.20) | copy-start | bytes 3145732
  0.7 8.3 %copy-start.6 = (f32[8,1,256]{2,1,0:T(1,128)S(1)}, f32[8,1,256]{2,1,0:T(1,128)}, u32[]{:S(2)}) copy-start(f32[8,1,256]{2,1,0:T(1,128)} %param.31) | copy-start | bytes 24580
  0.7 8.6 %copy-start.2 = (f32[8,1,256,256]{3,2,1,0:T(8,128)S(1)}, f32[8,1,256,256]{3,2,1,0:T(8,128)}, u32[]{:S(2)}) copy-start(f32[8,1,256,256]{3,2,1,0:T(8,128)} %param.30) | copy-start | bytes 6291460
  5.9 3.8 %copy-start.10 = (f32[8,1]{0,1:T(1,128)}, f32[8,1]{0,1:T(1,128)S(1)}, u32[]{:S(2)}) copy-start(f32[8,1]{0,1:T(1,128)S(1)} %get-tuple-element.29) | copy-start | bytes 100
  9.8 2.8 %copy-start.1 = (f32[8,1,256,256]{3,2,1,0:T(8,128)}, f32[8,1,256,256]{3,2,1,0:T(8,128)S(1)}, u32[]{:S(2)}) copy-start(f32[8,1,256,256]{3,2,1,0:T(8,128)S(1)} %multiply_add_fusion) | copy-start | bytes 6291460
  9.8 8.3 %copy-start.8 = (s32[8,4]{0,1:T(4,128)S(1)}, s32[8,4]{0,1:T(4,128)}, u32[]{:S(2)}) copy-start(s32[8,4]{0,1:T(4,128)} %param.36) | copy-start | bytes 388
  9.8 13.1 %copy-start.4 = (bf16[8,2048]{1,0:T(8,128)(2,1)S(1)}, bf16[8,2048]{1,0:T(8,128)(2,1)}, u32[]{:S(2)}) copy-start(bf16[8,2048]{1,0:T(8,128)(2,1)} %param.19) | copy-start | bytes 98308
  9.8 13.5 %copy-start.7 = (f32[2048]{0:T(1024)S(1)}, f32[2048]{0:T(1024)}, u32[]{:S(2)}) copy-start(f32[2048]{0:T(1024)} %param.29) | copy-start | bytes 24580
  13.3 9.7 %all-to-all-start = ((bf16[4,8,2048]{2,1,0:T(8,128)(2,1)}), bf16[4,8,2048]{2,1,0:T(8,128)(2,1)S(1)}, u32[]{:S(2)}, u32[]{:S(2)}) async-start(bf16[4,8,2048]{2,1,0:T(8,128)(2,1)} %broadcast_in_dim.13), calls=%async_computation | async-start | bytes 262144 | tf_op jit(solution)/shard_map/all_to_all | solution.py:11
  23.1 33.0 %copy-start.5 = (bf16[1,2048,128]{2,1,0:T(8,128)(2,1)S(1)}, bf16[1,2048,128]{2,1,0:T(8,128)(2,1)}, u32[]{:S(2)}) copy-start(bf16[1,2048,128]{2,1,0:T(8,128)(2,1)} %param.33) | copy-start | bytes 1572868
  58.3 24.4 %copy-start.9 = (f32[8,4]{0,1:T(4,128)S(1)}, f32[8,4]{0,1:T(4,128)}, u32[]{:S(2)}) copy-start(f32[8,4]{0,1:T(4,128)} %param.37) | copy-start | bytes 388
  76.4 17.3 %all-to-all-start.3 = ((bf16[64,2,512]{2,1,0:T(2,128)(2,1)}), bf16[64,2,512]{2,1,0:T(2,128)(2,1)S(1)}, u32[]{:S(2)}, u32[]{:S(2)}) async-start(bf16[64,2,512]{2,1,0:T(2,128)(2,1)} %copy.62), calls=%async_computation.3 | async-start | bytes 262144 | tf_op jit(solution)/shard_map/all_to_all | solution.py:131
where the time goes:
time: 95.8 us; the launch traced here: 95.2 us
  blocking collectives  48.5 us (51%)
  waiting for transfers between devices  14.5 us (15%)
  starting transfers between devices  11 us (11%)
  matrix products  9.84 us (10%)
  other arithmetic  5 us (5%)
  local copies, waits for them, and re-layouts  4.73 us (5%)
  between operations  1.55 us (2%)
    all_to_all x1, blocking collectives, shards(): lax.all_to_all(outbound, 'ep', split_axis=0, concat_axis=0, tiled=True)  31.2 us
    all_to_all x1, blocking collectives, sent_and_summed(): parts = lax.all_to_all(cut_along(value, dim, size), axis, 0, 0, tiled=True)  17.2 us
    all_to_all x1, waiting for transfers between devices, shards(): lax.all_to_all(reduced, 'ep', split_axis=0, concat_axis=0, tiled=True)  10.3 us
    all_to_all x1, starting transfers between devices, shards(): lax.all_to_all(reduced, 'ep', split_axis=0, concat_axis=0, tiled=True)  6.19 us
    all_to_all x1, starting transfers between devices, copy_for_each(): lax.all_to_all(jnp.broadcast_to(value[None], (size, *value.shape)), axis,...  4.83 us
    all_to_all x1, waiting for transfers between devices, copy_for_each(): lax.all_to_all(jnp.broadcast_to(value[None], (size, *value.shape)), axis,...  4.25 us
    dot_general x3, matrix products, shards(): jnp.dot(normed, weight, preferred_element_type=jnp.float32)  3.27 us
    dot_general x1, matrix products, shards(): jnp.dot(mixed, w_out, preferred_element_type=jnp.float32)  1.96 us
  transfers between devices with their start and end apart: 2, of which 2 were waited for; matrix products, arithmetic and copies ran while one was open for 1% of the time, Pallas kernels for 0%

commit v1 on v0

v1 whole, which is shorter than its diff:
```python
import functools

import jax
import jax.numpy as jnp
from jax import lax
from jax.experimental import pallas as pl
from jax.experimental.pallas import tpu as pltpu
from jax.sharding import PartitionSpec as P

F32 = jnp.float32
BF16 = jnp.bfloat16
MESH = pl.DeviceIdType.MESH

ROWS = 8
WIDTH = 2048
HEAD = 256
HIDDEN = 128
TOP = 4
NEP = 64
NTP = 4
CAP = 2
SLOTS = NEP * CAP
LANES = 128
CHUNKS = WIDTH // LANES
QUARTER = WIDTH // NTP
QCHUNKS = QUARTER // LANES
MSG = CHUNKS * CAP
QMSG = QCHUNKS * CAP
PITCH = 40
BIG = 1 << 20


def layer_norm(values, gain):
    mean = jnp.mean(values, -1, keepdims=True)
    centered = values - mean
    variance = jnp.mean(centered * centered, -1, keepdims=True)
    return centered * lax.rsqrt(variance + 1e-05) * gain


def iota(shape, dim):
    return lax.broadcasted_iota(jnp.int32, shape, dim)


def column(row, size):
    eye = iota((size, size), 0) == iota((size, size), 1)
    return jnp.sum(jnp.where(eye, row, 0.0), axis=1, keepdims=True)


def partner(me, k):
    a, b = k // 8, k % 8
    dz = 4 + (a // 2) * (1 - 2 * (a % 2)) - (a % 2)
    m = b // 2
    dy = 2 + (m // 2) * (1 - 2 * (m % 2)) - (m % 2)
    dc = 1 - b % 2
    z, y, c = me // 8, (me // 2) % 4, me % 2
    return (((z + dz) % 8) * 4 + (y + dy) % 4) * 2 + (c + dc) % 2


def kernel(
    tokens,
    gain_mix,
    gain_moe,
    w_igate,
    w_fgate,
    forget_bias,
    normalizer,
    stabilizer,
    routes,
    route_weight,
    w_key,
    w_value,
    w_query,
    w_outgate,
    memory,
    w_out,
    expert_gate,
    expert_up,
    expert_down,
    output,
    memory_next,
    norm_next,
    stabilizer_next,
    w_buf,
    mem_buf,
    out_buf,
    gu_buf,
    down_buf,
    num_buf,
    res_buf,
    heads,
    pick_buf,
    stage,
    disp_send,
    disp_recv,
    part_send,
    part_recv,
    ret_stage,
    ret_send,
    ret_recv,
    load_sem,
    store_sem,
    head_sems,
    disp_sems,
    part_sems,
    ret_sems,
):
    ep = lax.axis_index("ep")
    tp = lax.axis_index("tp")

    barrier = pltpu.get_barrier_semaphore()

    def greet(k, carry):
        pl.semaphore_signal(
            barrier, inc=1, device_id=(partner(ep, k), tp), device_id_type=MESH
        )
        return carry

    loads = [
        pltpu.make_async_copy(w, w_buf.at[i], load_sem.at[i])
        for i, w in enumerate((w_key, w_value, w_query, w_outgate))
    ]
    loads.append(pltpu.make_async_copy(memory.at[:, 0], mem_buf, load_sem.at[4]))
    loads.append(pltpu.make_async_copy(w_out, out_buf, load_sem.at[5]))
    loads.append(
        pltpu.make_async_copy(expert_gate.at[0], gu_buf.at[:, pl.ds(0, HIDDEN)], load_sem.at[6])
    )
    loads.append(
        pltpu.make_async_copy(
            expert_up.at[0], gu_buf.at[:, pl.ds(HIDDEN, HIDDEN)], load_sem.at[7]
        )
    )
    for q in range(NTP):
        loads.append(
            pltpu.make_async_copy(
                expert_down.at[0, :, pl.ds(q * QUARTER, QUARTER)],
                down_buf.at[q],
                load_sem.at[8 + q],
            )
        )
    for load in loads:
        load.start()

    lax.fori_loop(0, NEP - 1, greet, 0)
    for d in range(1, NTP):
        pl.semaphore_signal(
            barrier, inc=1, device_id=(ep, (tp + d) % NTP), device_id_type=MESH
        )

    token_rows = tokens[...].astype(F32)
    normed = layer_norm(token_rows, gain_mix[...]).astype(BF16)
    wide = normed.astype(F32)
    gate_in = jnp.sum(wide * w_igate[...].astype(F32), axis=1, keepdims=True)
    gate_forget = jnp.sum(wide * w_fgate[...].astype(F32), axis=1, keepdims=True)
    shifted = gate_forget + forget_bias[0]
    log_forget = jnp.minimum(shifted, 0.0) - jnp.log1p(jnp.exp(-jnp.abs(shifted)))
    carried = log_forget + column(stabilizer[...], ROWS)
    stab = jnp.maximum(carried, gate_in)
    keep = jnp.exp(carried - stab)
    admit = jnp.exp(gate_in - stab)
    eye = iota((ROWS, ROWS), 0) == iota((ROWS, ROWS), 1)
    stabilizer_next[...] = jnp.sum(jnp.where(eye, stab, 0.0), axis=0, keepdims=True)

    def project(i):
        loads[i].wait()
        product = jnp.dot(normed, w_buf[i], preferred_element_type=F32)
        return product.astype(BF16).astype(F32)

    keys = project(0) * (1.0 / 16.0)
    values = project(1)
    queries = project(2)
    admitted = admit * keys
    new_norm = keep * normalizer[:, 0, :] + admitted
    norm_next[:, 0, :] = new_norm
    denominator = jnp.sum(queries * new_norm, axis=1, keepdims=True)
    admitted_t = admitted.T
    queries_t = queries.T
    loads[4].wait()
    stores = []
    step = 64
    for s in range(ROWS):
        total = jnp.zeros((8, HEAD), F32)
        rate = keep[s : s + 1, :]
        value_row = values[s : s + 1, :]
        for r in range(0, HEAD, step):
            block = (
                rate * mem_buf[s, r : r + step, :]
                + admitted_t[r : r + step, s : s + 1] * value_row
            )
            mem_buf[s, r : r + step, :] = block
            weighed = queries_t[r : r + step, s : s + 1] * block
            total = total + jnp.sum(weighed.reshape(step // 8, 8, HEAD), axis=0)
        num_buf[s : s + 1, :] = jnp.sum(total, axis=0, keepdims=True)
        store = pltpu.make_async_copy(mem_buf.at[s], memory_next.at[s, 0], store_sem.at[s])
        store.start()
        stores.append(store)
    out_gate = project(3)
    readout = num_buf[...] / jnp.maximum(jnp.abs(denominator), jnp.exp(-stab))
    mixed = (readout / (1.0 + jnp.exp(-out_gate))).astype(BF16)
    loads[5].wait()
    heads[tp] = jnp.dot(mixed, out_buf[...], preferred_element_type=F32).astype(BF16)

    pl.semaphore_wait(barrier, NEP - 1 + NTP - 1)
    for d in range(1, NTP):
        pltpu.make_async_remote_copy(
            src_ref=heads.at[tp],
            dst_ref=heads.at[tp],
            send_sem=head_sems.at[0],
            recv_sem=head_sems.at[1],
            device_id=(ep, (tp + d) % NTP),
            device_id_type=MESH,
        ).start()

    route_rows = routes[...].astype(F32)
    earlier = iota((ROWS, ROWS), 0) < iota((ROWS, ROWS), 1)
    targets = []
    for choice in range(TOP):
        mine = route_rows[choice : choice + 1, :]
        same = jnp.zeros((ROWS, ROWS), F32)
        for other in range(TOP):
            theirs = column(route_rows[other : other + 1, :], ROWS)
            same = same + jnp.where((theirs == mine) & earlier, 1.0, 0.0)
        targets.append(mine * CAP + jnp.sum(same, axis=0, keepdims=True))
    spread = iota((ROWS, LANES), 1) % ROWS == iota((ROWS, LANES), 0)
    lane_chunk = (iota((1, LANES), 1) // ROWS).astype(F32)
    lane_keys = [
        jnp.sum(jnp.where(spread, column(t, ROWS), 0.0), axis=0, keepdims=True) * CHUNKS
        + lane_chunk
        for t in targets
    ]
    for part in range(8):
        height = NEP * MSG // 8
        row = iota((height, 1), 0) + part * height
        row_key = (
            ((row // MSG) * CAP + row % CAP) * CHUNKS + (row % MSG) // CAP
        ).astype(F32)
        hit = row_key == lane_keys[0]
        for lane_key in lane_keys[1:]:
            hit = hit | (row_key == lane_key)
        pick_buf[part * height : (part + 1) * height, :] = jnp.where(hit, 1.0, 0.0).astype(BF16)
    tall = NTP * ROWS
    copies = iota((tall, ROWS), 0) % ROWS == iota((tall, ROWS), 1)
    tall_chunk = (iota((tall, 1), 0) // ROWS).astype(F32)
    lane = iota((1, NEP * QMSG), 1)
    lane_key = (((lane // QMSG) * CAP + lane % CAP) * QCHUNKS + (lane % QMSG) // CAP).astype(F32)
    weigh = jnp.zeros((tall, NEP * QMSG), F32)
    for choice in range(TOP):
        tall_key = (
            jnp.sum(jnp.where(copies, targets[choice], 0.0), axis=1, keepdims=True) * QCHUNKS
            + tall_chunk
        )
        weight = jnp.sum(
            jnp.where(copies, route_weight[choice : choice + 1, :], 0.0), axis=1, keepdims=True
        )
        weigh = weigh + jnp.where(tall_key == lane_key, weight, 0.0)
    weigh_high = weigh.astype(BF16)
    weigh_low = (weigh - weigh_high.astype(F32)).astype(BF16)

    def arrivals(buffer, count, sems):
        return pltpu.make_async_remote_copy(
            src_ref=buffer.at[pl.ds(0, count)],
            dst_ref=buffer.at[pl.ds(0, count)],
            send_sem=sems.at[0],
            recv_sem=sems.at[1],
            device_id=(ep, tp),
            device_id_type=MESH,
        )

    arrivals(heads, NTP - 1, head_sems).wait_recv()
    summed = heads[0].astype(F32)
    for h in range(1, NTP):
        summed = summed + heads[h].astype(F32)
    residual = token_rows + summed
    for q in range(NTP):
        res_buf[q] = residual[:, q * QUARTER : (q + 1) * QUARTER]
    expert_in = layer_norm(residual, gain_moe[...])

    stacked = jnp.concatenate(
        [expert_in[:, j * LANES : (j + 1) * LANES] for j in range(CHUNKS)], axis=0
    ).astype(BF16)
    for part in range(8):
        height = NEP * MSG // 8
        picked = jnp.dot(
            pick_buf[part * height : (part + 1) * height, :],
            stacked,
            preferred_element_type=F32,
        ).astype(BF16)
        disp_send[part * 8 : (part + 1) * 8] = picked.reshape(8, MSG, LANES)

    def dispatch(k, carry):
        to = partner(ep, k)
        pltpu.make_async_remote_copy(
            src_ref=disp_send.at[to],
            dst_ref=disp_recv.at[ep],
            send_sem=disp_sems.at[0],
            recv_sem=disp_sems.at[1],
            device_id=(to, tp),
            device_id_type=MESH,
        ).start()
        return carry

    lax.fori_loop(0, NEP - 1, dispatch, 0)
    disp_recv[ep] = disp_send[ep]
    for load in loads[6:]:
        load.wait()
    arrivals(disp_recv, NEP - 1, disp_sems).wait_recv()

    for p in range(NEP):
        stage[p * PITCH : p * PITCH + MSG, :] = disp_recv[p].astype(F32)
    gate_up = jnp.zeros((SLOTS, 2 * HIDDEN), F32)
    for j in range(0, CHUNKS, 2):
        wide_rows = jnp.concatenate(
            [
                jnp.concatenate(
                    [stage[pl.ds((j + h) * CAP + c, NEP, stride=PITCH), :] for c in range(CAP)],
                    axis=0,
                )
                for h in range(2)
            ],
            axis=1,
        ).astype(BF16)
        gate_up = gate_up + jnp.dot(
            wide_rows, gu_buf[j * LANES : (j + 2) * LANES, :], preferred_element_type=F32
        )
    gate_part, up_part = gate_up[:, :HIDDEN], gate_up[:, HIDDEN:]
    hidden = (gate_part / (1.0 + jnp.exp(-gate_part)) * up_part).astype(BF16)

    for d in (2, 1, 3):
        to = (tp + d) % NTP
        part_send[d - 1] = jnp.dot(hidden, down_buf[to], preferred_element_type=F32).astype(BF16)
        pltpu.make_async_remote_copy(
            src_ref=part_send.at[d - 1],
            dst_ref=part_recv.at[d - 1],
            send_sem=part_sems.at[0],
            recv_sem=part_sems.at[1],
            device_id=(ep, to),
            device_id_type=MESH,
        ).start()
    own = jnp.dot(hidden, down_buf[tp], preferred_element_type=F32)
    arrivals(part_recv, NTP - 1, part_sems).wait_recv()
    for d in range(NTP - 1):
        own = own + part_recv[d].astype(F32)

    for j in range(QCHUNKS):
        for c in range(CAP):
            ret_stage[pl.ds(j * CAP + c, NEP, stride=QMSG), :] = own[
                c * NEP : (c + 1) * NEP, j * LANES : (j + 1) * LANES
            ]
    ret_send[...] = ret_stage[...].reshape(NEP, QMSG, LANES).astype(BF16)

    def give_back(k, carry):
        to = partner(ep, k)
        pltpu.make_async_remote_copy(
            src_ref=ret_send.at[to],
            dst_ref=ret_recv.at[ep],
            send_sem=ret_sems.at[0],
            recv_sem=ret_sems.at[1],
            device_id=(to, tp),
            device_id_type=MESH,
        ).start()
        return carry

    lax.fori_loop(0, NEP - 1, give_back, 0)
    ret_recv[ep] = ret_send[ep]
    for store in stores:
        store.wait()
    arrivals(heads, NTP - 1, head_sems).wait_send()
    arrivals(disp_recv, NEP - 1, disp_sems).wait_send()
    arrivals(part_recv, NTP - 1, part_sems).wait_send()
    arrivals(ret_recv, NEP - 1, ret_sems).wait_recv()
    returned = ret_recv[...].astype(F32).reshape(NEP * QMSG, LANES).astype(BF16)
    combined = jnp.dot(weigh_high, returned, preferred_element_type=F32) + jnp.dot(
        weigh_low, returned, preferred_element_type=F32
    )
    for j in range(QCHUNKS):
        output[:, j * LANES : (j + 1) * LANES] = (
            res_buf[tp, :, j * LANES : (j + 1) * LANES] + combined[j * ROWS : (j + 1) * ROWS]
        ).astype(BF16)
    arrivals(ret_recv, NEP - 1, ret_sems).wait_send()


def shards(
    tokens,
    w_query,
    w_key,
    w_value,
    w_outgate,
    w_igate,
    w_fgate,
    forget_bias,
    w_out,
    gain_mix,
    gain_moe,
    memory,
    normalizer,
    stabilizer,
    expert_gate,
    expert_up,
    expert_down,
    routes,
    route_weight,
):
    vmem = pl.BlockSpec(memory_space=pltpu.VMEM)
    smem = pl.BlockSpec(memory_space=pltpu.SMEM)
    hbm = pl.BlockSpec(memory_space=pl.ANY)
    output, memory_next, norm_next, stab = pl.pallas_call(
        kernel,
        out_shape=(
            jax.ShapeDtypeStruct((ROWS, QUARTER), BF16),
            jax.ShapeDtypeStruct(memory.shape, F32),
            jax.ShapeDtypeStruct(normalizer.shape, F32),
            jax.ShapeDtypeStruct((1, ROWS), F32),
        ),
        in_specs=[vmem] * 5 + [smem] + [vmem] * 4 + [hbm] * 9,
        out_specs=(vmem, hbm, vmem, vmem),
        scratch_shapes=[
            pltpu.VMEM((4, WIDTH, HEAD), BF16),
            pltpu.VMEM((ROWS, HEAD, HEAD), F32),
            pltpu.VMEM((HEAD, WIDTH), BF16),
            pltpu.VMEM((WIDTH, 2 * HIDDEN), BF16),
            pltpu.VMEM((NTP, HIDDEN, QUARTER), BF16),
            pltpu.VMEM((ROWS, HEAD), F32),
            pltpu.VMEM((NTP, ROWS, QUARTER), F32),
            pltpu.VMEM((NTP, ROWS, WIDTH), BF16),
            pltpu.VMEM((NEP * MSG, LANES), BF16),
            pltpu.VMEM((NEP * PITCH, LANES), F32),
            pltpu.VMEM((NEP, MSG, LANES), BF16),
            pltpu.VMEM((NEP, MSG, LANES), BF16),
            pltpu.VMEM((NTP - 1, SLOTS, QUARTER), BF16),
            pltpu.VMEM((NTP - 1, SLOTS, QUARTER), BF16),
            pltpu.VMEM((NEP * QMSG, LANES), F32),
            pltpu.VMEM((NEP, QMSG, LANES), BF16),
            pltpu.VMEM((NEP, QMSG, LANES), BF16),
            pltpu.SemaphoreType.DMA((12,)),
            pltpu.SemaphoreType.DMA((ROWS,)),
            pltpu.SemaphoreType.DMA((2,)),
            pltpu.SemaphoreType.DMA((2,)),
            pltpu.SemaphoreType.DMA((2,)),
            pltpu.SemaphoreType.DMA((2,)),
        ],
        compiler_params=pltpu.CompilerParams(
            collective_id=0, has_side_effects=True, vmem_limit_bytes=60 * 1024 * 1024
        ),
        name="layer",
    )(
        tokens,
        gain_mix.reshape(1, WIDTH),
        gain_moe.reshape(1, WIDTH),
        w_igate.reshape(1, WIDTH),
        w_fgate.reshape(1, WIDTH),
        forget_bias,
        normalizer,
        stabilizer.reshape(1, ROWS),
        routes.T,
        route_weight.T,
        w_key,
        w_value,
        w_query,
        w_outgate,
        memory,
        w_out,
        expert_gate,
        expert_up,
        expert_down,
    )
    return output, memory_next, norm_next, stab.reshape(ROWS, 1)


def solution(mesh):
    return jax.shard_map(
        shards,
        mesh=mesh,
        in_specs=(
            P("ep", None),
            P(None, "tp"),
            P(None, "tp"),
            P(None, "tp"),
            P(None, "tp"),
            P(None, "tp"),
            P(None, "tp"),
            P("tp"),
            P("tp", None),
            P(),
            P(),
            P("ep", "tp", None, None),
            P("ep", "tp", None),
            P("ep", "tp"),
            P("ep", None, "tp"),
            P("ep", None, "tp"),
            P("ep", "tp", None),
            P("ep", None),
            P("ep", None),
        ),
        out_specs=(P("ep", "tp"), P("ep", "tp", None, None), P("ep", "tp", None), P("ep", "tp")),
        check_vma=False,
    )
```

time: 95.8 us -> 55.2 us (0.58)
  blocking collectives: 48.5 us -> 0 us
  Pallas kernels: 0 us -> 48.2 us
  waiting for transfers between devices: 14.5 us -> 0 us
  starting transfers between devices: 11 us -> 0 us
  matrix products: 9.84 us -> 0 us
  other arithmetic: 5 us -> 0 us
    all_to_all x2 -> x0, blocking collectives: 48.5 us -> none  [the longest x1 31.2 us: shards(): lax.all_to_all(outbound, 'ep', split_axis=0, concat_axis=0, tiled=True)]
    pallas_call x0 -> x1, Pallas kernels: none -> 48.2 us  [shards(): pl.pallas_call(kernel, out_shape=(jax.ShapeDtypeStruct((ROWS, QUARTER), B...]
    all_to_all x2 -> x0, waiting for transfers between devices: 14.5 us -> none  [the longest x1 10.3 us: shards(): lax.all_to_all(reduced, 'ep', split_axis=0, concat_axis=0, tiled=True)]
    all_to_all x2 -> x0, starting transfers between devices: 11 us -> none  [the longest x1 6.19 us: shards(): lax.all_to_all(reduced, 'ep', split_axis=0, concat_axis=0, tiled=True)]
    dot_general x9 -> x0, matrix products: 9.84 us -> none  [the longest x3 3.27 us: shards(): jnp.dot(normed, weight, preferred_element_type=jnp.float32)]
    unnamed x25 -> x8, local copies, waits for them, and re-layouts: 0.88 us -> 5.47 us
    reduce_sum x8 -> x0, other arithmetic: 2.81 us -> none  [the longest x2 1.22 us: layer_norm(): variance = jnp.mean(centered * centered, -1, keepdims=True)]
    convert_element_type x4 -> x0, other arithmetic: 1.6 us -> none  [the longest x1 0.84 us: shards(): normed = layer_norm(tokens, gain_mix).astype(jnp.bfloat16)]
  transfers between devices with their start and end apart: 2 -> 0, of which waited for: 2 -> 0; matrix products, arithmetic and copies ran while one was open for 1% -> 0% of each run, Pallas kernels for 0% -> 0%
where the time goes in v1:
time: 55.2 us; the launch traced here: 54.9 us
  Pallas kernels  48.2 us (87%)
  local copies, waits for them, and re-layouts  5.47 us (10%)
  between operations  1.3 us (2%)
    pallas_call x1, Pallas kernels, shards(): pl.pallas_call(kernel, out_shape=(jax.ShapeDtypeStruct((ROWS, QUARTER), B...  48.2 us
    unnamed x8, local copies, waits for them, and re-layouts  5.47 us

profile of v1, /device:TPU:1, one launch (start us, length us, event | category | flops | bytes accessed | tf_op | source)
XLA Modules:
  0.0 54.9 jit_solution(1951279849813236268)
XLA Ops:
  1.3 48.2 %layer.1 = (bf16[8,512]{1,0:T(8,128)(2,1)}, f32[8,1,256,256]{3,2,1,0:T(8,128)}, f32[8,1,256]{2,1,0:T(1,128)}, f32[1,8]{1,0:T(1,128)}) custom-call(bf16[8,2048]{1,0:T(8,128)(2,1)} %tokens.1, f32[1,2048]{1,0:T(1,128)} %bitcast.8, f32[1,2048]{1,0:T(1,128)} %bitcast.9, bf16[1,2048]{1,0:T(2,128)(2,1)} %bitcast.10, bf16[1,2048]{1,0:T(2,128)(2,1)} %bitcast.11, ...), custom_call_target="tpu_custom_call" | custom-call | tf_op jit(solution)/shard_map/layer/pallas_call | solution.py:405
  49.4 1.3 %copy.28 = bf16[8,512]{1,0:T(8,128)(2,1)} copy(bf16[8,512]{1,0:T(8,128)(2,1)} %get-tuple-element.16) | data formatting | bytes 16384
  50.7 0.0 copy-start
  50.7 0.0 copy-start.1
  50.7 3.1 %copy.29 = f32[8,1,256,256]{3,2,1,0:T(8,128)} copy(f32[8,1,256,256]{3,2,1,0:T(8,128)} %get-tuple-element.17) | data formatting | bytes 4194304
  53.8 0.0 copy-done
  53.8 0.6 %copy.30 = f32[8,1,256]{2,1,0:T(1,128)} copy(f32[8,1,256]{2,1,0:T(1,128)S(1)} %copy-done) | data formatting | bytes 16384
  54.4 0.0 copy-done.1
  54.4 0.5 copy.31
Async XLA Ops:
  50.7 3.1 %copy-start = (f32[8,1,256]{2,1,0:T(1,128)S(1)}, f32[8,1,256]{2,1,0:T(1,128)}, u32[]{:S(2)}) copy-start(f32[8,1,256]{2,1,0:T(1,128)} %get-tuple-element.18) | copy-start | bytes 24580
  50.7 3.7 %copy-start.1 = (f32[1,8]{1,0:T(1,128)S(1)}, f32[1,8]{1,0:T(1,128)}, u32[]{:S(2)}) copy-start(f32[1,8]{1,0:T(1,128)} %get-tuple-element.11) | copy-start | bytes 100

commit v2 on v1

v2 whole, which is shorter than its diff:
```python
import functools

import jax
import jax.numpy as jnp
from jax import lax
from jax.experimental import pallas as pl
from jax.experimental.pallas import tpu as pltpu
from jax.sharding import PartitionSpec as P

F32 = jnp.float32
BF16 = jnp.bfloat16
MESH = pl.DeviceIdType.MESH

ROWS = 8
WIDTH = 2048
HEAD = 256
HIDDEN = 128
TOP = 4
NEP = 64
NTP = 4
CAP = 2
SLOTS = NEP * CAP
LANES = 128
QUARTER = WIDTH // NTP
QCHUNKS = QUARTER // LANES
QMSG = QCHUNKS * CAP
HALF = NEP // 2


def layer_norm(values, gain):
    mean = jnp.mean(values, -1, keepdims=True)
    centered = values - mean
    variance = jnp.mean(centered * centered, -1, keepdims=True)
    return centered * lax.rsqrt(variance + 1e-05) * gain


def iota(shape, dim):
    return lax.broadcasted_iota(jnp.int32, shape, dim)


def column(row, size):
    eye = iota((size, size), 0) == iota((size, size), 1)
    return jnp.sum(jnp.where(eye, row, 0.0), axis=1, keepdims=True)


def ring_step(k, middle):
    return middle + (k // 2) * (1 - 2 * (k % 2)) - k % 2


def each_partner(ep, sign, first, last, act):
    z, y, c = ep // 8, (ep // 2) % 4, ep % 2
    columns = [
        ((y + sign * ring_step(m, 2) + 4) % 4) * 2 + (c + sign * dc + 2) % 2
        for m in range(4)
        for dc in (1, 0)
    ]

    def plane(a, count):
        base = ((z + sign * ring_step(a, 4) + 8) % 8) * 8
        for b in range(count):
            act(a * 8 + b, base + columns[b])

    def whole(a, carry):
        plane(a, 8)
        return carry

    if last == NEP:
        lax.fori_loop(first // 8, last // 8 - 1, whole, 0)
        plane(NEP // 8 - 1, 7)
    else:
        lax.fori_loop(first // 8, last // 8, whole, 0)


def kernel(
    tokens_in,
    gain_mix_in,
    gain_moe_in,
    w_igate_in,
    w_fgate_in,
    normalizer_in,
    stabilizer_in,
    routes_in,
    route_weight_in,
    w_key,
    w_value,
    w_query,
    w_outgate,
    memory,
    w_out,
    expert_gate,
    expert_up,
    expert_down,
    forget_bias,
    output,
    admitted_out,
    values_out,
    keep_out,
    norm_next,
    stabilizer_next,
    tokens,
    gain_mix,
    gain_moe,
    w_igate,
    w_fgate,
    normalizer,
    stabilizer,
    routes,
    route_weight,
    w_buf,
    mem_buf,
    out_buf,
    gu_buf,
    down_buf,
    num_buf,
    res_buf,
    in_buf,
    heads,
    stage,
    disp_send,
    rows,
    part_send,
    part_recv,
    ret_stage,
    ret_send,
    ret_recv,
    small_sem,
    load_sem,
    head_sems,
    disp_sems,
    row_sems,
    part_sems,
    ret_sems,
):
    ep = lax.axis_index("ep")
    tp = lax.axis_index("tp")

    smalls = [
        pltpu.make_async_copy(source, target, small_sem.at[i])
        for i, (source, target) in enumerate(
            (
                (tokens_in, tokens),
                (gain_mix_in, gain_mix),
                (w_igate_in, w_igate),
                (w_fgate_in, w_fgate),
                (stabilizer_in, stabilizer),
                (normalizer_in, normalizer),
                (gain_moe_in, gain_moe),
                (routes_in, routes),
                (route_weight_in, route_weight),
            )
        )
    ]
    loads = [
        pltpu.make_async_copy(w, w_buf.at[i], load_sem.at[i])
        for i, w in enumerate((w_key, w_value, w_query, w_outgate))
    ]
    loads.append(pltpu.make_async_copy(memory.at[:, 0], mem_buf, load_sem.at[4]))
    loads.append(pltpu.make_async_copy(w_out, out_buf, load_sem.at[5]))
    loads.append(
        pltpu.make_async_copy(expert_gate.at[0], gu_buf.at[:, pl.ds(0, HIDDEN)], load_sem.at[6])
    )
    loads.append(
        pltpu.make_async_copy(
            expert_up.at[0], gu_buf.at[:, pl.ds(HIDDEN, HIDDEN)], load_sem.at[7]
        )
    )
    for q in range(NTP):
        loads.append(
            pltpu.make_async_copy(
                expert_down.at[0, :, pl.ds(q * QUARTER, QUARTER)],
                down_buf.at[q],
                load_sem.at[8 + q],
            )
        )
    for load in smalls + loads:
        load.start()

    barrier = pltpu.get_barrier_semaphore()

    def greet(k, index):
        pl.semaphore_signal(barrier, inc=1, device_id=(index, tp), device_id_type=MESH)

    each_partner(ep, 1, 0, NEP, greet)
    for d in range(1, NTP):
        pl.semaphore_signal(
            barrier, inc=1, device_id=(ep, (tp + d) % NTP), device_id_type=MESH
        )

    for small in smalls[:6]:
        small.wait()
    token_rows = tokens[...].astype(F32)
    normed = layer_norm(token_rows, gain_mix[...]).astype(BF16)
    wide = normed.astype(F32)
    gate_in = jnp.sum(wide * w_igate[...].astype(F32), axis=1, keepdims=True)
    gate_forget = jnp.sum(wide * w_fgate[...].astype(F32), axis=1, keepdims=True)
    shifted = gate_forget + forget_bias[0]
    log_forget = jnp.minimum(shifted, 0.0) - jnp.log1p(jnp.exp(-jnp.abs(shifted)))
    carried = log_forget + column(stabilizer[...], ROWS)
    stab = jnp.maximum(carried, gate_in)
    keep = jnp.exp(carried - stab)
    admit = jnp.exp(gate_in - stab)
    eye = iota((ROWS, ROWS), 0) == iota((ROWS, ROWS), 1)
    stabilizer_next[...] = jnp.sum(jnp.where(eye, stab, 0.0), axis=0, keepdims=True)

    def project(i):
        loads[i].wait()
        product = jnp.dot(normed, w_buf[i], preferred_element_type=F32)
        return product.astype(BF16).astype(F32)

    keys = project(0) * (1.0 / 16.0)
    values = project(1)
    queries = project(2)
    admitted = admit * keys
    new_norm = keep * normalizer[:, 0, :] + admitted
    norm_next[:, 0, :] = new_norm
    admitted_out[...] = admitted
    values_out[...] = values
    keep_out[...] = jnp.broadcast_to(keep, (ROWS, LANES))
    denominator = jnp.sum(queries * new_norm, axis=1, keepdims=True)
    admitted_t = admitted.T
    queries_t = queries.T
    loads[4].wait()
    step = 64
    for s in range(ROWS):
        total = jnp.zeros((8, HEAD), F32)
        rate = keep[s : s + 1, :]
        value_row = values[s : s + 1, :]
        for r in range(0, HEAD, step):
            block = (
                rate * mem_buf[s, r : r + step, :]
                + admitted_t[r : r + step, s : s + 1] * value_row
            )
            weighed = queries_t[r : r + step, s : s + 1] * block
            total = total + jnp.sum(weighed.reshape(step // 8, 8, HEAD), axis=0)
        num_buf[s : s + 1, :] = jnp.sum(total, axis=0, keepdims=True)
    out_gate = project(3)
    readout = num_buf[...] / jnp.maximum(jnp.abs(denominator), jnp.exp(-stab))
    mixed = (readout / (1.0 + jnp.exp(-out_gate))).astype(BF16)
    loads[5].wait()
    heads[tp] = jnp.dot(mixed, out_buf[...], preferred_element_type=F32).astype(BF16)

    pl.semaphore_wait(barrier, NEP - 1 + NTP - 1)
    for d in (2, 1, 3):
        pltpu.make_async_remote_copy(
            src_ref=heads.at[tp],
            dst_ref=heads.at[tp],
            send_sem=head_sems.at[0],
            recv_sem=head_sems.at[1],
            device_id=(ep, (tp + d) % NTP),
            device_id_type=MESH,
        ).start()

    for small in smalls[6:]:
        small.wait()
    route_rows = routes[...].astype(F32)
    earlier = iota((ROWS, ROWS), 0) < iota((ROWS, ROWS), 1)
    targets = []
    for choice in range(TOP):
        mine = route_rows[choice : choice + 1, :]
        same = jnp.zeros((ROWS, ROWS), F32)
        for other in range(TOP):
            theirs = column(route_rows[other : other + 1, :], ROWS)
            same = same + jnp.where((theirs == mine) & earlier, 1.0, 0.0)
        targets.append(mine * CAP + jnp.sum(same, axis=0, keepdims=True))
    tall = QCHUNKS * ROWS
    copies = iota((tall, ROWS), 0) % ROWS == iota((tall, ROWS), 1)
    tall_chunk = (iota((tall, 1), 0) // ROWS).astype(F32)
    lane = iota((1, NEP * QMSG), 1)
    lane_key = (((lane // QMSG) * CAP + lane % CAP) * QCHUNKS + (lane % QMSG) // CAP).astype(F32)
    weigh = jnp.zeros((tall, NEP * QMSG), F32)
    filled = jnp.zeros((tall, NEP * QMSG), F32)
    for choice in range(TOP):
        tall_key = (
            jnp.sum(jnp.where(copies, targets[choice], 0.0), axis=1, keepdims=True) * QCHUNKS
            + tall_chunk
        )
        weight = jnp.sum(
            jnp.where(copies, route_weight[choice : choice + 1, :], 0.0), axis=1, keepdims=True
        )
        hit = tall_key == lane_key
        weigh = weigh + jnp.where(hit, weight, 0.0)
        filled = filled + jnp.where(hit, 1.0, 0.0)
    weigh_high = weigh.astype(BF16)
    weigh_low = (weigh - weigh_high.astype(F32)).astype(BF16)
    pick = filled.T.astype(BF16)

    def bytes_of(view, sems):
        return pltpu.make_async_remote_copy(
            src_ref=view,
            dst_ref=view,
            send_sem=sems.at[0],
            recv_sem=sems.at[1],
            device_id=(ep, tp),
            device_id_type=MESH,
        )

    bytes_of(heads.at[pl.ds(0, NTP - 1)], head_sems).wait_recv()
    summed = heads[0].astype(F32)
    for h in range(1, NTP):
        summed = summed + heads[h].astype(F32)
    residual = token_rows + summed
    expert_in = layer_norm(residual, gain_moe[...])
    for q in range(NTP):
        res_buf[q] = residual[:, q * QUARTER : (q + 1) * QUARTER]
        in_buf[q] = expert_in[:, q * QUARTER : (q + 1) * QUARTER]

    stacked = jnp.concatenate(
        [in_buf[tp, :, j * LANES : (j + 1) * LANES] for j in range(QCHUNKS)], axis=0
    ).astype(BF16)
    picked = jnp.dot(pick, stacked, preferred_element_type=F32).astype(BF16)
    disp_send[...] = picked.reshape(NEP, QMSG, LANES)

    def dispatch(group):
        def send(k, to):
            pltpu.make_async_remote_copy(
                src_ref=disp_send.at[to],
                dst_ref=rows.at[tp, k],
                send_sem=disp_sems.at[group, 0],
                recv_sem=disp_sems.at[group, 1],
                device_id=(to, tp),
                device_id_type=MESH,
            ).start()

        each_partner(ep, 1, group * HALF, (group + 1) * HALF, send)

    dispatch(0)
    dispatch(1)
    rows[tp, NEP - 1] = disp_send[ep]

    def spread(group):
        block = pl.ds(group * HALF, HALF)
        bytes_of(
            rows.at[0, pl.ds(group * HALF, HALF - group)], disp_sems.at[group]
        ).wait_recv()
        for d in (2, 1, 3):
            pltpu.make_async_remote_copy(
                src_ref=rows.at[tp, block],
                dst_ref=rows.at[tp, block],
                send_sem=row_sems.at[group, 0],
                recv_sem=row_sems.at[group, 1],
                device_id=(ep, (tp + d) % NTP),
                device_id_type=MESH,
            ).start()

    def spread_bytes(group):
        return bytes_of(
            rows.at[pl.ds(0, NTP - 1), pl.ds(group * HALF, HALF)], row_sems.at[group]
        )

    def expert(group):
        spread_bytes(group).wait_recv()
        height = HALF * QMSG
        for q in range(NTP):
            stage[q * height : (q + 1) * height, :] = (
                rows[q, group * HALF : (group + 1) * HALF].astype(F32).reshape(height, LANES)
            )
        gate_up = jnp.zeros((HALF * CAP, 2 * HIDDEN), F32)
        for q in range(NTP):
            for j in range(0, QCHUNKS, 2):
                wide_rows = jnp.concatenate(
                    [
                        jnp.concatenate(
                            [
                                stage[
                                    pl.ds(q * height + (j + h) * CAP + c, HALF, stride=QMSG), :
                                ]
                                for c in range(CAP)
                            ],
                            axis=0,
                        )
                        for h in range(2)
                    ],
                    axis=1,
                ).astype(BF16)
                first = q * QUARTER + j * LANES
                gate_up = gate_up + jnp.dot(
                    wide_rows, gu_buf[first : first + 2 * LANES, :], preferred_element_type=F32
                )
        gate_part, up_part = gate_up[:, :HIDDEN], gate_up[:, HIDDEN:]
        hidden = (gate_part / (1.0 + jnp.exp(-gate_part)) * up_part).astype(BF16)
        for d in (2, 1, 3):
            to = (tp + d) % NTP
            part_send[group, d - 1] = jnp.dot(
                hidden, down_buf[to], preferred_element_type=F32
            ).astype(BF16)
            pltpu.make_async_remote_copy(
                src_ref=part_send.at[group, d - 1],
                dst_ref=part_recv.at[group, d - 1],
                send_sem=part_sems.at[group, 0],
                recv_sem=part_sems.at[group, 1],
                device_id=(ep, to),
                device_id_type=MESH,
            ).start()
        return jnp.dot(hidden, down_buf[tp], preferred_element_type=F32)

    def give_back(group, own):
        bytes_of(part_recv.at[group], part_sems.at[group]).wait_recv()
        for d in range(NTP - 1):
            own = own + part_recv[group, d].astype(F32)
        for j in range(QCHUNKS):
            for c in range(CAP):
                ret_stage[pl.ds(j * CAP + c, HALF, stride=QMSG), :] = own[
                    c * HALF : (c + 1) * HALF, j * LANES : (j + 1) * LANES
                ]
        ret_send[group * HALF : (group + 1) * HALF] = (
            ret_stage[...].reshape(HALF, QMSG, LANES).astype(BF16)
        )

        def send(k, to):
            pltpu.make_async_remote_copy(
                src_ref=ret_send.at[k],
                dst_ref=ret_recv.at[ep],
                send_sem=ret_sems.at[0],
                recv_sem=ret_sems.at[1],
                device_id=(to, tp),
                device_id_type=MESH,
            ).start()

        each_partner(ep, -1, group * HALF, (group + 1) * HALF, send)

    spread(1)
    spread(0)
    for load in loads[6:]:
        load.wait()
    near = expert(1)
    far = expert(0)
    give_back(1, near)
    give_back(0, far)
    ret_recv[ep] = ret_send[NEP - 1]
    bytes_of(heads.at[pl.ds(0, NTP - 1)], head_sems).wait_send()
    for group in range(2):
        bytes_of(
            rows.at[0, pl.ds(group * HALF, HALF - group)], disp_sems.at[group]
        ).wait_send()
        spread_bytes(group).wait_send()
        bytes_of(part_recv.at[group], part_sems.at[group]).wait_send()
    everything = bytes_of(ret_recv.at[pl.ds(0, NEP - 1)], ret_sems)
    everything.wait_recv()
    returned = ret_recv[...].astype(F32).reshape(NEP * QMSG, LANES).astype(BF16)
    combined = jnp.dot(weigh_high, returned, preferred_element_type=F32) + jnp.dot(
        weigh_low, returned, preferred_element_type=F32
    )
    for j in range(QCHUNKS):
        output[:, j * LANES : (j + 1) * LANES] = (
            res_buf[tp, :, j * LANES : (j + 1) * LANES] + combined[j * ROWS : (j + 1) * ROWS]
        ).astype(BF16)
    everything.wait_send()


def update_kernel(
    admitted_in,
    values_in,
    keep_in,
    memory,
    output_in,
    norm_in,
    stab_in,
    memory_next,
    output,
    norm_next,
    stabilizer_next,
    admitted,
    values,
    keep,
    mem_buf,
    output_buf,
    norm_buf,
    stab_buf,
    load_sem,
    store_sem,
):
    loads = [
        pltpu.make_async_copy(source, target, load_sem.at[i])
        for i, (source, target) in enumerate(
            (
                (admitted_in, admitted),
                (values_in, values),
                (keep_in, keep),
                (output_in, output_buf),
                (norm_in, norm_buf),
                (stab_in, stab_buf),
            )
        )
    ]
    blocks = [
        pltpu.make_async_copy(memory.at[s, 0], mem_buf.at[s], load_sem.at[6 + s])
        for s in range(ROWS)
    ]
    for load in loads + blocks:
        load.start()
    passed = [
        pltpu.make_async_copy(source, target, store_sem.at[ROWS + i])
        for i, (source, target) in enumerate(
            ((output_buf, output), (norm_buf, norm_next), (stab_buf, stabilizer_next))
        )
    ]
    for load in loads[:3]:
        load.wait()
    admitted_t = admitted[...].T
    for load, store in zip(loads[3:], passed, strict=True):
        load.wait()
        store.start()
    stores = []
    for s in range(ROWS):
        blocks[s].wait()
        mem_buf[s] = (
            keep[s : s + 1, 0:1] * mem_buf[s] + admitted_t[:, s : s + 1] * values[s : s + 1, :]
        )
        store = pltpu.make_async_copy(mem_buf.at[s], memory_next.at[s, 0], store_sem.at[s])
        store.start()
        stores.append(store)
    for store in passed + stores:
        store.wait()


def shards(
    tokens,
    w_query,
    w_key,
    w_value,
    w_outgate,
    w_igate,
    w_fgate,
    forget_bias,
    w_out,
    gain_mix,
    gain_moe,
    memory,
    normalizer,
    stabilizer,
    expert_gate,
    expert_up,
    expert_down,
    routes,
    route_weight,
):
    vmem = pl.BlockSpec(memory_space=pltpu.VMEM)
    smem = pl.BlockSpec(memory_space=pltpu.SMEM)
    hbm = pl.BlockSpec(memory_space=pl.ANY)
    smalls = (
        tokens,
        gain_mix.reshape(1, WIDTH),
        gain_moe.reshape(1, WIDTH),
        w_igate.reshape(1, WIDTH),
        w_fgate.reshape(1, WIDTH),
        normalizer,
        stabilizer.reshape(1, ROWS),
        routes.T,
        route_weight.T,
    )
    norm_shape = jax.ShapeDtypeStruct(normalizer.shape, F32)
    output_shape = jax.ShapeDtypeStruct((ROWS, QUARTER), BF16)
    stab_shape = jax.ShapeDtypeStruct((1, ROWS), F32)
    row_shape = jax.ShapeDtypeStruct((ROWS, HEAD), F32)
    keep_shape = jax.ShapeDtypeStruct((ROWS, LANES), F32)
    message = (QMSG, LANES)
    output, admitted, values, keep, norm_next, stab = pl.pallas_call(
        kernel,
        out_shape=(output_shape, row_shape, row_shape, keep_shape, norm_shape, stab_shape),
        in_specs=[hbm] * 18 + [smem],
        out_specs=(vmem,) * 6,
        scratch_shapes=[pltpu.VMEM(x.shape, x.dtype) for x in smalls]
        + [
            pltpu.VMEM((4, WIDTH, HEAD), BF16),
            pltpu.VMEM((ROWS, HEAD, HEAD), F32),
            pltpu.VMEM((HEAD, WIDTH), BF16),
            pltpu.VMEM((WIDTH, 2 * HIDDEN), BF16),
            pltpu.VMEM((NTP, HIDDEN, QUARTER), BF16),
            pltpu.VMEM((ROWS, HEAD), F32),
            pltpu.VMEM((NTP, ROWS, QUARTER), F32),
            pltpu.VMEM((NTP, ROWS, QUARTER), F32),
            pltpu.VMEM((NTP, ROWS, WIDTH), BF16),
            pltpu.VMEM((NTP * HALF * QMSG, LANES), F32),
            pltpu.VMEM((NEP, *message), BF16),
            pltpu.VMEM((NTP, NEP, *message), BF16),
            pltpu.VMEM((2, NTP - 1, HALF * CAP, QUARTER), BF16),
            pltpu.VMEM((2, NTP - 1, HALF * CAP, QUARTER), BF16),
            pltpu.VMEM((HALF * QMSG, LANES), F32),
            pltpu.VMEM((NEP, *message), BF16),
            pltpu.VMEM((NEP, *message), BF16),
            pltpu.SemaphoreType.DMA((9,)),
            pltpu.SemaphoreType.DMA((12,)),
            pltpu.SemaphoreType.DMA((2,)),
            pltpu.SemaphoreType.DMA((2, 2)),
            pltpu.SemaphoreType.DMA((2, 2)),
            pltpu.SemaphoreType.DMA((2, 2)),
            pltpu.SemaphoreType.DMA((2,)),
        ],
        compiler_params=pltpu.CompilerParams(
            collective_id=0, has_side_effects=True, vmem_limit_bytes=60 * 1024 * 1024
        ),
        name="layer",
    )(
        *smalls,
        w_key,
        w_value,
        w_query,
        w_outgate,
        memory,
        w_out,
        expert_gate,
        expert_up,
        expert_down,
        forget_bias,
    )
    memory_next, output, norm_next, stab = pl.pallas_call(
        update_kernel,
        out_shape=(
            jax.ShapeDtypeStruct(memory.shape, F32),
            output_shape,
            norm_shape,
            stab_shape,
        ),
        in_specs=[hbm] * 7,
        out_specs=(hbm,) * 4,
        scratch_shapes=[
            pltpu.VMEM((ROWS, HEAD), F32),
            pltpu.VMEM((ROWS, HEAD), F32),
            pltpu.VMEM((ROWS, LANES), F32),
            pltpu.VMEM((ROWS, HEAD, HEAD), F32),
            pltpu.VMEM(output_shape.shape, BF16),
            pltpu.VMEM(norm_shape.shape, F32),
            pltpu.VMEM(stab_shape.shape, F32),
            pltpu.SemaphoreType.DMA((6 + ROWS,)),
            pltpu.SemaphoreType.DMA((ROWS + 3,)),
        ],
        compiler_params=pltpu.CompilerParams(vmem_limit_bytes=60 * 1024 * 1024),
        name="update",
    )(admitted, values, keep, memory, output, norm_next, stab)
    return output, memory_next, norm_next, stab.reshape(ROWS, 1)


def solution(mesh):
    return jax.shard_map(
        shards,
        mesh=mesh,
        in_specs=(
            P("ep", None),
            P(None, "tp"),
            P(None, "tp"),
            P(None, "tp"),
            P(None, "tp"),
            P(None, "tp"),
            P(None, "tp"),
            P("tp"),
            P("tp", None),
            P(),
            P(),
            P("ep", "tp", None, None),
            P("ep", "tp", None),
            P("ep", "tp"),
            P("ep", None, "tp"),
            P("ep", None, "tp"),
            P("ep", "tp", None),
            P("ep", None),
            P("ep", None),
        ),
        out_specs=(P("ep", "tp"), P("ep", "tp", None, None), P("ep", "tp", None), P("ep", "tp")),
        check_vma=False,
    )
```

time: 55.2 us -> 48.2 us (0.87)
  local copies, waits for them, and re-layouts: 5.47 us -> 0 us
  Pallas kernels: 48.2 us -> 46.7 us
    unnamed x8 -> x0, local copies, waits for them, and re-layouts: 5.47 us -> none
    pallas_call x1 -> x2, Pallas kernels: 48.2 us -> 46.7 us  [the longest x1 43.9 us: shards(): pl.pallas_call(kernel, out_shape=(output_shape, row_shape, row_shape, kee...]
where the time goes in v2:
time: 48.2 us; the launch traced here: 48 us
  Pallas kernels  46.7 us (97%)
  between operations  1.29 us (3%)
    pallas_call x1, Pallas kernels, shards(): pl.pallas_call(kernel, out_shape=(output_shape, row_shape, row_shape, kee...  43.9 us
    pallas_call x1, Pallas kernels, shards(): pl.pallas_call(update_kernel, out_shape=(jax.ShapeDtypeStruct(memory.shap...  2.84 us

profile of v2, /device:TPU:1, one launch (start us, length us, event | category | flops | bytes accessed | tf_op | source)
XLA Modules:
  0.0 48.0 jit_solution(7742126194127030654)
XLA Ops:
  1.3 43.9 %layer.1 = (bf16[8,512]{1,0:T(8,128)(2,1)}, f32[8,256]{1,0:T(8,128)}, f32[8,256]{1,0:T(8,128)}, f32[8,128]{1,0:T(8,128)}, f32[8,1,256]{2,1,0:T(1,128)}, /*index=5*/f32[1,8]{1,0:T(1,128)}) custom-call(bf16[8,2048]{1,0:T(8,128)(2,1)} %tokens_in.1, f32[1,2048]{1,0:T(1,128)} %bitcast.8, f32[1,2048]{1,0:T(1,128)} %bitcast.9, bf16[1,2048]{1,0:T(2,128)(2,1)} %bitcast.10, ...), custom_call_target="tpu_custom_call" | custom-call | tf_op jit(solution)/shard_map/layer/pallas_call | solution.py:557
  45.2 2.8 %update.1 = (f32[8,1,256,256]{3,2,1,0:T(8,128)}, bf16[8,512]{1,0:T(8,128)(2,1)}, f32[8,1,256]{2,1,0:T(1,128)}, f32[1,8]{1,0:T(1,128)}) custom-call(f32[8,256]{1,0:T(8,128)} %get-tuple-element.14.admitted_in, f32[8,256]{1,0:T(8,128)} %get-tuple-element.15.values_in, f32[8,128]{1,0:T(8,128)} %get-tuple-element.16.keep_in, f32[8,1,256,256]{3,2,1,0:T(8,128)} %memory.3, ...), custom_call_target="tpu_custom_call" | custom-call | tf_op jit(solution)/shard_map/update/pallas_call | solution.py:606

commit v3 on v2

--- a/solution.py
+++ b/solution.py
@@ -24,7 +24,8 @@
 QUARTER = WIDTH // NTP
 QCHUNKS = QUARTER // LANES
 QMSG = QCHUNKS * CAP
-HALF = NEP // 2
+GROUPS = 4
+GROUP = NEP // GROUPS
 
 
 def layer_norm(values, gain):
@@ -43,32 +44,34 @@
     return jnp.sum(jnp.where(eye, row, 0.0), axis=1, keepdims=True)
 
 
-def ring_step(k, middle):
-    return middle + (k // 2) * (1 - 2 * (k % 2)) - k % 2
-
-
-def each_partner(ep, sign, first, last, act):
+def ring_step(k):
+    return (k // 2) * (1 - 2 * (k % 2)) - k % 2
+
+
+def each_partner(ep, sign, first, last, act, far_first=False):
     z, y, c = ep // 8, (ep // 2) % 4, ep % 2
     columns = [
-        ((y + sign * ring_step(m, 2) + 4) % 4) * 2 + (c + sign * dc + 2) % 2
+        ((y + sign * ring_step(m) + 4) % 4) * 2 + (c + sign * dc + 2) % 2
         for m in range(4)
-        for dc in (1, 0)
+        for dc in (0, 1)
     ]
-
-    def plane(a, count):
-        base = ((z + sign * ring_step(a, 4) + 8) % 8) * 8
-        for b in range(count):
+    low, high = max(first // 8, 1), last // 8
+
+    def plane(a, start):
+        base = ((z + sign * ring_step(a) + 8) % 8) * 8
+        order = range(7, start - 1, -1) if far_first else range(start, 8)
+        for b in order:
             act(a * 8 + b, base + columns[b])
 
-    def whole(a, carry):
-        plane(a, 8)
+    def whole(i, carry):
+        plane(low + high - 1 - i if far_first else i, 0)
         return carry
 
-    if last == NEP:
-        lax.fori_loop(first // 8, last // 8 - 1, whole, 0)
-        plane(NEP // 8 - 1, 7)
-    else:
-        lax.fori_loop(first // 8, last // 8, whole, 0)
+    if first == 0 and not far_first:
+        plane(0, 1)
+    lax.fori_loop(low, high, whole, 0)
+    if first == 0 and far_first:
+        plane(0, 1)
 
 
 def kernel(
@@ -117,6 +120,7 @@
     heads,
     stage,
     disp_send,
+    disp_opposite,
     rows,
     part_send,
     part_recv,
@@ -157,11 +161,11 @@
     loads.append(pltpu.make_async_copy(memory.at[:, 0], mem_buf, load_sem.at[4]))
     loads.append(pltpu.make_async_copy(w_out, out_buf, load_sem.at[5]))
     loads.append(
-        pltpu.make_async_copy(expert_gate.at[0], gu_buf.at[:, pl.ds(0, HIDDEN)], load_sem.at[6])
+        pltpu.make_async_copy(expert_gate, gu_buf.at[:, :, pl.ds(0, HIDDEN)], load_sem.at[6])
     )
     loads.append(
         pltpu.make_async_copy(
-            expert_up.at[0], gu_buf.at[:, pl.ds(HIDDEN, HIDDEN)], load_sem.at[7]
+            expert_up, gu_buf.at[:, :, pl.ds(HIDDEN, HIDDEN)], load_sem.at[7]
         )
     )
     for q in range(NTP):
@@ -172,15 +176,19 @@
                 load_sem.at[8 + q],
             )
         )
-    for load in smalls + loads:
-        load.start()
+    for small in smalls:
+        small.start()
 
     barrier = pltpu.get_barrier_semaphore()
+    opposite = (tp + 2) % NTP
 
     def greet(k, index):
         pl.semaphore_signal(barrier, inc=1, device_id=(index, tp), device_id_type=MESH)
 
-    each_partner(ep, 1, 0, NEP, greet)
+    each_partner(ep, 1, NEP // 2, NEP, greet, far_first=True)
+    for i in (0, 1, 2, 4, 3, 5):
+        loads[i].start()
+    each_partner(ep, 1, 0, NEP // 2, greet, far_first=True)
     for d in range(1, NTP):
         pl.semaphore_signal(
             barrier, inc=1, device_id=(ep, (tp + d) % NTP), device_id_type=MESH
@@ -250,6 +258,9 @@
             device_id_type=MESH,
         ).start()
 
+    for load in loads[6:]:
+        load.start()
+
     for small in smalls[6:]:
         small.wait()
     route_rows = routes[...].astype(F32)
@@ -304,35 +315,47 @@
         res_buf[q] = residual[:, q * QUARTER : (q + 1) * QUARTER]
         in_buf[q] = expert_in[:, q * QUARTER : (q + 1) * QUARTER]
 
-    stacked = jnp.concatenate(
-        [in_buf[tp, :, j * LANES : (j + 1) * LANES] for j in range(QCHUNKS)], axis=0
-    ).astype(BF16)
-    picked = jnp.dot(pick, stacked, preferred_element_type=F32).astype(BF16)
-    disp_send[...] = picked.reshape(NEP, QMSG, LANES)
-
-    def dispatch(group):
+    def pick_quarter(q):
+        stacked = jnp.concatenate(
+            [in_buf[q, :, j * LANES : (j + 1) * LANES] for j in range(QCHUNKS)], axis=0
+        ).astype(BF16)
+        picked = jnp.dot(pick, stacked, preferred_element_type=F32).astype(BF16)
+        return picked.reshape(NEP, QMSG, LANES)
+
+    def dispatch(first, last, source, q, sems, far_first):
         def send(k, to):
             pltpu.make_async_remote_copy(
-                src_ref=disp_send.at[to],
-                dst_ref=rows.at[tp, k],
-                send_sem=disp_sems.at[group, 0],
-                recv_sem=disp_sems.at[group, 1],
+                src_ref=source.at[to],
+                dst_ref=rows.at[q, k],
+                send_sem=sems.at[0],
+                recv_sem=sems.at[1],
                 device_id=(to, tp),
                 device_id_type=MESH,
             ).start()
 
-        each_partner(ep, 1, group * HALF, (group + 1) * HALF, send)
-
-    dispatch(0)
-    dispatch(1)
-    rows[tp, NEP - 1] = disp_send[ep]
-
-    def spread(group):
-        block = pl.ds(group * HALF, HALF)
-        bytes_of(
-            rows.at[0, pl.ds(group * HALF, HALF - group)], disp_sems.at[group]
-        ).wait_recv()
-        for d in (2, 1, 3):
+        each_partner(ep, 1, first, last, send, far_first)
+
+    disp_send[...] = pick_quarter(tp)
+    for group in range(GROUPS):
+        dispatch(group * GROUP, (group + 1) * GROUP, disp_send, tp, disp_sems.at[group], False)
+    rows[tp, 0] = disp_send[ep]
+    disp_opposite[...] = pick_quarter(opposite)
+
+    neighbours = (1, NTP - 1)
+    others = (2, 1, NTP - 1)
+
+    def own_bytes(group):
+        return bytes_of(
+            rows.at[0, pl.ds(0, GROUP - (group == 0))], disp_sems.at[group]
+        )
+
+    def spread_bytes(group):
+        return bytes_of(rows.at[pl.ds(0, 2), pl.ds(group * GROUP, GROUP)], row_sems.at[group])
+
+    for group in range(GROUPS):
+        own_bytes(group).wait_recv()
+        block = pl.ds(group * GROUP, GROUP)
+        for d in neighbours:
             pltpu.make_async_remote_copy(
                 src_ref=rows.at[tp, block],
                 dst_ref=rows.at[tp, block],
@@ -341,101 +364,120 @@
                 device_id=(ep, (tp + d) % NTP),
                 device_id_type=MESH,
             ).start()
-
-    def spread_bytes(group):
-        return bytes_of(
-            rows.at[pl.ds(0, NTP - 1), pl.ds(group * HALF, HALF)], row_sems.at[group]
-        )
-
-    def expert(group):
+        if group == 0:
+            dispatch(0, NEP, disp_opposite, opposite, disp_sems.at[GROUPS], True)
+            rows[opposite, 0] = disp_opposite[ep]
+
+    for load in loads[6:]:
+        load.wait()
+    height = NEP * QMSG
+    quarters = []
+
+    def absorb(i, q):
+        stage[i * height : (i + 1) * height, :] = rows[q].astype(F32).reshape(height, LANES)
+        product = jnp.zeros((SLOTS, 2 * HIDDEN), F32)
+        for j in range(0, QCHUNKS, 2):
+            wide_rows = jnp.concatenate(
+                [
+                    jnp.concatenate(
+                        [
+                            stage[
+                                pl.ds(
+                                    i * height + group * GROUP * QMSG + (j + h) * CAP + c,
+                                    GROUP,
+                                    stride=QMSG,
+                                ),
+                                :,
+                            ]
+                            for group in range(GROUPS)
+                            for c in range(CAP)
+                        ],
+                        axis=0,
+                    )
+                    for h in range(2)
+                ],
+                axis=1,
+            ).astype(BF16)
+            product = product + jnp.dot(
+                wide_rows, gu_buf[q, j * LANES : (j + 2) * LANES, :], preferred_element_type=F32
+            )
+        quarters.append(product)
+
+    opposite_bytes = bytes_of(rows.at[0, pl.ds(0, NEP - 1)], disp_sems.at[GROUPS])
+    absorb(0, tp)
+    opposite_bytes.wait_recv()
+    absorb(1, opposite)
+    for group in range(GROUPS):
         spread_bytes(group).wait_recv()
-        height = HALF * QMSG
-        for q in range(NTP):
-            stage[q * height : (q + 1) * height, :] = (
-                rows[q, group * HALF : (group + 1) * HALF].astype(F32).reshape(height, LANES)
-            )
-        gate_up = jnp.zeros((HALF * CAP, 2 * HIDDEN), F32)
-        for q in range(NTP):
-            for j in range(0, QCHUNKS, 2):
-                wide_rows = jnp.concatenate(
-                    [
-                        jnp.concatenate(
-                            [
-                                stage[
-                                    pl.ds(q * height + (j + h) * CAP + c, HALF, stride=QMSG), :
-                                ]
-                                for c in range(CAP)
-                            ],
-                            axis=0,
-                        )
-                        for h in range(2)
-                    ],
-                    axis=1,
-                ).astype(BF16)
-                first = q * QUARTER + j * LANES
-                gate_up = gate_up + jnp.dot(
-                    wide_rows, gu_buf[first : first + 2 * LANES, :], preferred_element_type=F32
+    absorb(2, (tp + 1) % NTP)
+    absorb(3, (tp + 3) % NTP)
+    gate_up = (quarters[0] + quarters[1]) + (quarters[2] + quarters[3])
+    gate_part, up_part = gate_up[:, :HIDDEN], gate_up[:, HIDDEN:]
+    hidden = (gate_part / (1.0 + jnp.exp(-gate_part)) * up_part).astype(BF16)
+
+    def partial(q):
+        return jnp.dot(hidden, down_buf[q], preferred_element_type=F32)
+
+    def send_part(group, i):
+        pltpu.make_async_remote_copy(
+            src_ref=part_send.at[group, i],
+            dst_ref=part_recv.at[group, i],
+            send_sem=part_sems.at[group, 0],
+            recv_sem=part_sems.at[group, 1],
+            device_id=(ep, (tp + others[i]) % NTP),
+            device_id_type=MESH,
+        ).start()
+
+    for i in range(NTP - 1):
+        product = partial((tp + others[i]) % NTP).astype(BF16)
+        for group in range(GROUPS):
+            part_send[group, i] = product[group * GROUP * CAP : (group + 1) * GROUP * CAP]
+        send_part(GROUPS - 1, i)
+    for group in range(GROUPS - 2, -1, -1):
+        for i in range(NTP - 1):
+            send_part(group, i)
+
+    def as_messages(product, group):
+        for j in range(QCHUNKS):
+            for c in range(CAP):
+                ret_stage[pl.ds(group * GROUP * QMSG + j * CAP + c, GROUP, stride=QMSG), :] = (
+                    product[c * GROUP : (c + 1) * GROUP, j * LANES : (j + 1) * LANES]
                 )
-        gate_part, up_part = gate_up[:, :HIDDEN], gate_up[:, HIDDEN:]
-        hidden = (gate_part / (1.0 + jnp.exp(-gate_part)) * up_part).astype(BF16)
-        for d in (2, 1, 3):
-            to = (tp + d) % NTP
-            part_send[group, d - 1] = jnp.dot(
-                hidden, down_buf[to], preferred_element_type=F32
-            ).astype(BF16)
+        block = ret_stage[group * GROUP * QMSG : (group + 1) * GROUP * QMSG, :]
+        return block.reshape(GROUP, QMSG, LANES).astype(BF16)
+
+    def return_to(source, target, sems, lane_of_tp):
+        def send(k, to):
             pltpu.make_async_remote_copy(
-                src_ref=part_send.at[group, d - 1],
-                dst_ref=part_recv.at[group, d - 1],
-                send_sem=part_sems.at[group, 0],
-                recv_sem=part_sems.at[group, 1],
-                device_id=(ep, to),
+                src_ref=source.at[k],
+                dst_ref=target.at[ep],
+                send_sem=sems.at[0],
+                recv_sem=sems.at[1],
+                device_id=(to, lane_of_tp),
                 device_id_type=MESH,
             ).start()
-        return jnp.dot(hidden, down_buf[tp], preferred_element_type=F32)
-
-    def give_back(group, own):
+
+        return send
+
+    own = partial(tp)
+    send_own = return_to(ret_send, ret_recv, ret_sems, tp)
+    for group in range(GROUPS - 1, -1, -1):
         bytes_of(part_recv.at[group], part_sems.at[group]).wait_recv()
-        for d in range(NTP - 1):
-            own = own + part_recv[group, d].astype(F32)
-        for j in range(QCHUNKS):
-            for c in range(CAP):
-                ret_stage[pl.ds(j * CAP + c, HALF, stride=QMSG), :] = own[
-                    c * HALF : (c + 1) * HALF, j * LANES : (j + 1) * LANES
-                ]
-        ret_send[group * HALF : (group + 1) * HALF] = (
-            ret_stage[...].reshape(HALF, QMSG, LANES).astype(BF16)
-        )
-
-        def send(k, to):
-            pltpu.make_async_remote_copy(
-                src_ref=ret_send.at[k],
-                dst_ref=ret_recv.at[ep],
-                send_sem=ret_sems.at[0],
-                recv_sem=ret_sems.at[1],
-                device_id=(to, tp),
-                device_id_type=MESH,
-            ).start()
-
-        each_partner(ep, -1, group * HALF, (group + 1) * HALF, send)
-
-    spread(1)
-    spread(0)
-    for load in loads[6:]:
-        load.wait()
-    near = expert(1)
-    far = expert(0)
-    give_back(1, near)
-    give_back(0, far)
-    ret_recv[ep] = ret_send[NEP - 1]
+        total = own[group * GROUP * CAP : (group + 1) * GROUP * CAP]
+        for i in range(NTP - 1):
+            total = total + part_recv[group, i].astype(F32)
+        ret_send[group * GROUP : (group + 1) * GROUP] = as_messages(total, group)
+        each_partner(ep, -1, group * GROUP, (group + 1) * GROUP, send_own, True)
+    ret_recv[ep] = ret_send[0]
+
     bytes_of(heads.at[pl.ds(0, NTP - 1)], head_sems).wait_send()
-    for group in range(2):
-        bytes_of(
-            rows.at[0, pl.ds(group * HALF, HALF - group)], disp_sems.at[group]
-        ).wait_send()
+    for group in range(GROUPS):
+        own_bytes(group).wait_send()
         spread_bytes(group).wait_send()
         bytes_of(part_recv.at[group], part_sems.at[group]).wait_send()
-    everything = bytes_of(ret_recv.at[pl.ds(0, NEP - 1)], ret_sems)
-    everything.wait_recv()
+    opposite_bytes.wait_send()
+    from_own = bytes_of(ret_recv.at[pl.ds(0, NEP - 1)], ret_sems)
+    from_own.wait_recv()
     returned = ret_recv[...].astype(F32).reshape(NEP * QMSG, LANES).astype(BF16)
     combined = jnp.dot(weigh_high, returned, preferred_element_type=F32) + jnp.dot(
         weigh_low, returned, preferred_element_type=F32
@@ -444,7 +486,7 @@
         output[:, j * LANES : (j + 1) * LANES] = (
             res_buf[tp, :, j * LANES : (j + 1) * LANES] + combined[j * ROWS : (j + 1) * ROWS]
         ).astype(BF16)
-    everything.wait_send()
+    from_own.wait_send()
 
 
 def update_kernel(
@@ -564,26 +606,27 @@
             pltpu.VMEM((4, WIDTH, HEAD), BF16),
             pltpu.VMEM((ROWS, HEAD, HEAD), F32),
             pltpu.VMEM((HEAD, WIDTH), BF16),
-            pltpu.VMEM((WIDTH, 2 * HIDDEN), BF16),
+            pltpu.VMEM((NTP, QUARTER, 2 * HIDDEN), BF16),
             pltpu.VMEM((NTP, HIDDEN, QUARTER), BF16),
             pltpu.VMEM((ROWS, HEAD), F32),
             pltpu.VMEM((NTP, ROWS, QUARTER), F32),
             pltpu.VMEM((NTP, ROWS, QUARTER), F32),
             pltpu.VMEM((NTP, ROWS, WIDTH), BF16),
-            pltpu.VMEM((NTP * HALF * QMSG, LANES), F32),
+            pltpu.VMEM((NTP * NEP * QMSG, LANES), F32),
+            pltpu.VMEM((NEP, *message), BF16),
             pltpu.VMEM((NEP, *message), BF16),
             pltpu.VMEM((NTP, NEP, *message), BF16),
-            pltpu.VMEM((2, NTP - 1, HALF * CAP, QUARTER), BF16),
-            pltpu.VMEM((2, NTP - 1, HALF * CAP, QUARTER), BF16),
-            pltpu.VMEM((HALF * QMSG, LANES), F32),
+            pltpu.VMEM((GROUPS, NTP - 1, GROUP * CAP, QUARTER), BF16),
+            pltpu.VMEM((GROUPS, NTP - 1, GROUP * CAP, QUARTER), BF16),
+            pltpu.VMEM((NEP * QMSG, LANES), F32),
             pltpu.VMEM((NEP, *message), BF16),
             pltpu.VMEM((NEP, *message), BF16),
             pltpu.SemaphoreType.DMA((9,)),
             pltpu.SemaphoreType.DMA((12,)),
             pltpu.SemaphoreType.DMA((2,)),
-            pltpu.SemaphoreType.DMA((2, 2)),
-            pltpu.SemaphoreType.DMA((2, 2)),
-            pltpu.SemaphoreType.DMA((2, 2)),
+            pltpu.SemaphoreType.DMA((GROUPS + 1, 2)),
+            pltpu.SemaphoreType.DMA((GROUPS, 2)),
+            pltpu.SemaphoreType.DMA((GROUPS, 2)),
             pltpu.SemaphoreType.DMA((2,)),
         ],
         compiler_params=pltpu.CompilerParams(
@@ -598,8 +641,8 @@
         w_outgate,
         memory,
         w_out,
-        expert_gate,
-        expert_up,
+        expert_gate.reshape(NTP, QUARTER, HIDDEN),
+        expert_up.reshape(NTP, QUARTER, HIDDEN),
         expert_down,
         forget_bias,
     )

time: 48.2 us -> 45.6 us (0.946)
  Pallas kernels: 46.7 us -> 44.1 us
    pallas_call x1, Pallas kernels: 43.9 us -> 41.3 us  [shards(): pl.pallas_call(kernel, out_shape=(output_shape, row_shape, row_shape, kee...]
where the time goes in v3:
time: 45.6 us; the launch traced here: 45.4 us
  Pallas kernels  44.1 us (97%)
  between operations  1.29 us (3%)
    pallas_call x1, Pallas kernels, shards(): pl.pallas_call(kernel, out_shape=(output_shape, row_shape, row_shape, kee...  41.3 us
    pallas_call x1, Pallas kernels, shards(): pl.pallas_call(update_kernel, out_shape=(jax.ShapeDtypeStruct(memory.shap...  2.84 us

profile of v3, /device:TPU:1, one launch (start us, length us, event | category | flops | bytes accessed | tf_op | source)
XLA Modules:
  0.0 45.4 jit_solution(4174420752960060306)
XLA Ops:
  1.3 41.3 %layer.1 = (bf16[8,512]{1,0:T(8,128)(2,1)}, f32[8,256]{1,0:T(8,128)}, f32[8,256]{1,0:T(8,128)}, f32[8,128]{1,0:T(8,128)}, f32[8,1,256]{2,1,0:T(1,128)}, /*index=5*/f32[1,8]{1,0:T(1,128)}) custom-call(bf16[8,2048]{1,0:T(8,128)(2,1)} %tokens_in.1, f32[1,2048]{1,0:T(1,128)} %bitcast.12, f32[1,2048]{1,0:T(1,128)} %bitcast.13, bf16[1,2048]{1,0:T(2,128)(2,1)} %bitcast.14, ...), custom_call_target="tpu_custom_call" | custom-call | tf_op jit(solution)/shard_map/layer/pallas_call | solution.py:599
  42.6 2.8 %update.1 = (f32[8,1,256,256]{3,2,1,0:T(8,128)}, bf16[8,512]{1,0:T(8,128)(2,1)}, f32[8,1,256]{2,1,0:T(1,128)}, f32[1,8]{1,0:T(1,128)}) custom-call(f32[8,256]{1,0:T(8,128)} %get-tuple-element.14.admitted_in, f32[8,256]{1,0:T(8,128)} %get-tuple-element.15.values_in, f32[8,128]{1,0:T(8,128)} %get-tuple-element.16.keep_in, f32[8,1,256,256]{3,2,1,0:T(8,128)} %memory.3, ...), custom_call_target="tpu_custom_call" | custom-call | tf_op jit(solution)/shard_map/update/pallas_call | solution.py:649

commit v4 on v3

--- a/solution.py
+++ b/solution.py
@@ -94,6 +94,12 @@
     expert_up,
     expert_down,
     forget_bias,
+    output_hbm,
+    admitted_hbm,
+    values_hbm,
+    keep_hbm,
+    norm_hbm,
+    stabilizer_hbm,
     output,
     admitted_out,
     values_out,
@@ -127,6 +133,10 @@
     ret_stage,
     ret_send,
     ret_recv,
+    opp_send,
+    opp_recv,
+    cross_send,
+    cross_recv,
     small_sem,
     load_sem,
     head_sems,
@@ -134,6 +144,7 @@
     row_sems,
     part_sems,
     ret_sems,
+    out_sem,
 ):
     ep = lax.axis_index("ep")
     tp = lax.axis_index("tp")
@@ -186,8 +197,8 @@
         pl.semaphore_signal(barrier, inc=1, device_id=(index, tp), device_id_type=MESH)
 
     each_partner(ep, 1, NEP // 2, NEP, greet, far_first=True)
-    for i in (0, 1, 2, 4, 3, 5):
-        loads[i].start()
+    for load in loads[:3]:
+        load.start()
     each_partner(ep, 1, 0, NEP // 2, greet, far_first=True)
     for d in range(1, NTP):
         pl.semaphore_signal(
@@ -215,7 +226,10 @@
         product = jnp.dot(normed, w_buf[i], preferred_element_type=F32)
         return product.astype(BF16).astype(F32)
 
+    loads[4].start()
     keys = project(0) * (1.0 / 16.0)
+    loads[3].start()
+    loads[5].start()
     values = project(1)
     queries = project(2)
     admitted = admit * keys
@@ -261,6 +275,22 @@
     for load in loads[6:]:
         load.start()
 
+    stores = [
+        pltpu.make_async_copy(source, target, out_sem.at[i])
+        for i, (source, target) in enumerate(
+            (
+                (output, output_hbm),
+                (admitted_out, admitted_hbm),
+                (values_out, values_hbm),
+                (keep_out, keep_hbm),
+                (norm_next, norm_hbm),
+                (stabilizer_next, stabilizer_hbm),
+            )
+        )
+    ]
+    for store in stores[1:]:
+        store.start()
+
     for small in smalls[6:]:
         small.wait()
     route_rows = routes[...].astype(F32)
@@ -342,7 +372,6 @@
     disp_opposite[...] = pick_quarter(opposite)
 
     neighbours = (1, NTP - 1)
-    others = (2, 1, NTP - 1)
 
     def own_bytes(group):
         return bytes_of(
@@ -424,17 +453,17 @@
             dst_ref=part_recv.at[group, i],
             send_sem=part_sems.at[group, 0],
             recv_sem=part_sems.at[group, 1],
-            device_id=(ep, (tp + others[i]) % NTP),
+            device_id=(ep, (tp + neighbours[i]) % NTP),
             device_id_type=MESH,
         ).start()
 
-    for i in range(NTP - 1):
-        product = partial((tp + others[i]) % NTP).astype(BF16)
+    for i in range(2):
+        product = partial((tp + neighbours[i]) % NTP).astype(BF16)
         for group in range(GROUPS):
             part_send[group, i] = product[group * GROUP * CAP : (group + 1) * GROUP * CAP]
         send_part(GROUPS - 1, i)
     for group in range(GROUPS - 2, -1, -1):
-        for i in range(NTP - 1):
+        for i in range(2):
             send_part(group, i)
 
     def as_messages(product, group):
@@ -459,34 +488,67 @@
 
         return send
 
+    product = partial(opposite)
+    for group in range(GROUPS):
+        opp_send[group * GROUP : (group + 1) * GROUP] = as_messages(
+            product[group * GROUP * CAP : (group + 1) * GROUP * CAP], group
+        )
+    each_partner(ep, -1, 0, NEP, return_to(opp_send, opp_recv, ret_sems.at[1], tp), True)
+    opp_recv[ep] = opp_send[0]
+
     own = partial(tp)
-    send_own = return_to(ret_send, ret_recv, ret_sems, tp)
+    send_own = return_to(ret_send, ret_recv, ret_sems.at[0], tp)
     for group in range(GROUPS - 1, -1, -1):
         bytes_of(part_recv.at[group], part_sems.at[group]).wait_recv()
         total = own[group * GROUP * CAP : (group + 1) * GROUP * CAP]
-        for i in range(NTP - 1):
+        for i in range(2):
             total = total + part_recv[group, i].astype(F32)
         ret_send[group * GROUP : (group + 1) * GROUP] = as_messages(total, group)
         each_partner(ep, -1, group * GROUP, (group + 1) * GROUP, send_own, True)
     ret_recv[ep] = ret_send[0]
 
+
+    def weighted(buffer):
+        returned = buffer[...].astype(F32).reshape(NEP * QMSG, LANES).astype(BF16)
+        return jnp.dot(weigh_high, returned, preferred_element_type=F32) + jnp.dot(
+            weigh_low, returned, preferred_element_type=F32
+        )
+
+    back = [
+        bytes_of(buffer.at[pl.ds(0, NEP - 1)], ret_sems.at[i])
+        for i, buffer in enumerate((ret_recv, opp_recv))
+    ]
+    back[1].wait_recv()
+    cross_send[...] = weighted(opp_recv)
+    cross = pltpu.make_async_remote_copy(
+        src_ref=cross_send,
+        dst_ref=cross_recv,
+        send_sem=ret_sems.at[2, 0],
+        recv_sem=ret_sems.at[2, 1],
+        device_id=(ep, opposite),
+        device_id_type=MESH,
+    )
+    cross.start()
     bytes_of(heads.at[pl.ds(0, NTP - 1)], head_sems).wait_send()
     for group in range(GROUPS):
         own_bytes(group).wait_send()
         spread_bytes(group).wait_send()
         bytes_of(part_recv.at[group], part_sems.at[group]).wait_send()
     opposite_bytes.wait_send()
-    from_own = bytes_of(ret_recv.at[pl.ds(0, NEP - 1)], ret_sems)
-    from_own.wait_recv()
-    returned = ret_recv[...].astype(F32).reshape(NEP * QMSG, LANES).astype(BF16)
-    combined = jnp.dot(weigh_high, returned, preferred_element_type=F32) + jnp.dot(
-        weigh_low, returned, preferred_element_type=F32
-    )
+    back[0].wait_recv()
+    combined = weighted(ret_recv)
+    cross.wait_recv()
+    combined = combined + cross_recv[...]
     for j in range(QCHUNKS):
         output[:, j * LANES : (j + 1) * LANES] = (
             res_buf[tp, :, j * LANES : (j + 1) * LANES] + combined[j * ROWS : (j + 1) * ROWS]
         ).astype(BF16)
-    from_own.wait_send()
+    stores[0].start()
+    cross.wait_send()
+    for messages in back:
+        messages.wait_send()
+    for store in stores:
+        store.wait()
 
 
 def update_kernel(
@@ -596,12 +658,13 @@
     row_shape = jax.ShapeDtypeStruct((ROWS, HEAD), F32)
     keep_shape = jax.ShapeDtypeStruct((ROWS, LANES), F32)
     message = (QMSG, LANES)
+    results = (output_shape, row_shape, row_shape, keep_shape, norm_shape, stab_shape)
     output, admitted, values, keep, norm_next, stab = pl.pallas_call(
         kernel,
-        out_shape=(output_shape, row_shape, row_shape, keep_shape, norm_shape, stab_shape),
+        out_shape=results,
         in_specs=[hbm] * 18 + [smem],
-        out_specs=(vmem,) * 6,
-        scratch_shapes=[pltpu.VMEM(x.shape, x.dtype) for x in smalls]
+        out_specs=(hbm,) * 6,
+        scratch_shapes=[pltpu.VMEM(x.shape, x.dtype) for x in (*results, *smalls)]
         + [
             pltpu.VMEM((4, WIDTH, HEAD), BF16),
             pltpu.VMEM((ROWS, HEAD, HEAD), F32),
@@ -616,18 +679,23 @@
             pltpu.VMEM((NEP, *message), BF16),
             pltpu.VMEM((NEP, *message), BF16),
             pltpu.VMEM((NTP, NEP, *message), BF16),
-            pltpu.VMEM((GROUPS, NTP - 1, GROUP * CAP, QUARTER), BF16),
-            pltpu.VMEM((GROUPS, NTP - 1, GROUP * CAP, QUARTER), BF16),
+            pltpu.VMEM((GROUPS, 2, GROUP * CAP, QUARTER), BF16),
+            pltpu.VMEM((GROUPS, 2, GROUP * CAP, QUARTER), BF16),
             pltpu.VMEM((NEP * QMSG, LANES), F32),
             pltpu.VMEM((NEP, *message), BF16),
             pltpu.VMEM((NEP, *message), BF16),
+            pltpu.VMEM((NEP, *message), BF16),
+            pltpu.VMEM((NEP, *message), BF16),
+            pltpu.VMEM((QCHUNKS * ROWS, LANES), F32),
+            pltpu.VMEM((QCHUNKS * ROWS, LANES), F32),
             pltpu.SemaphoreType.DMA((9,)),
             pltpu.SemaphoreType.DMA((12,)),
             pltpu.SemaphoreType.DMA((2,)),
             pltpu.SemaphoreType.DMA((GROUPS + 1, 2)),
             pltpu.SemaphoreType.DMA((GROUPS, 2)),
             pltpu.SemaphoreType.DMA((GROUPS, 2)),
-            pltpu.SemaphoreType.DMA((2,)),
+            pltpu.SemaphoreType.DMA((3, 2)),
+            pltpu.SemaphoreType.DMA((6,)),
         ],
         compiler_params=pltpu.CompilerParams(
             collective_id=0, has_side_effects=True, vmem_limit_bytes=60 * 1024 * 1024

time: 45.6 us -> 43.3 us (0.950)
  Pallas kernels: 44.1 us -> 41.8 us
    pallas_call x1, Pallas kernels: 41.3 us -> 39 us  [shards(): pl.pallas_call(kernel, out_shape=results, in_specs=[hbm] * 18 + [smem], o...]
where the time goes in v4:
time: 43.3 us; the launch traced here: 43.1 us
  Pallas kernels  41.8 us (97%)
  between operations  1.29 us (3%)
    pallas_call x1, Pallas kernels, shards(): pl.pallas_call(kernel, out_shape=results, in_specs=[hbm] * 18 + [smem], o...  39 us
    pallas_call x1, Pallas kernels, shards(): pl.pallas_call(update_kernel, out_shape=(jax.ShapeDtypeStruct(memory.shap...  2.84 us

profile of v4, /device:TPU:1, one launch (start us, length us, event | category | flops | bytes accessed | tf_op | source)
XLA Modules:
  0.0 43.1 jit_solution(1031260982786121883)
XLA Ops:
  1.3 39.0 %layer.1 = (bf16[8,512]{1,0:T(8,128)(2,1)}, f32[8,256]{1,0:T(8,128)}, f32[8,256]{1,0:T(8,128)}, f32[8,128]{1,0:T(8,128)}, f32[8,1,256]{2,1,0:T(1,128)}, /*index=5*/f32[1,8]{1,0:T(1,128)}) custom-call(bf16[8,2048]{1,0:T(8,128)(2,1)} %tokens_in.1, f32[1,2048]{1,0:T(1,128)} %bitcast.12, f32[1,2048]{1,0:T(1,128)} %bitcast.13, bf16[1,2048]{1,0:T(2,128)(2,1)} %bitcast.14, ...), custom_call_target="tpu_custom_call" | custom-call | tf_op jit(solution)/shard_map/layer/pallas_call | solution.py:662
  40.3 2.8 %update.1 = (f32[8,1,256,256]{3,2,1,0:T(8,128)}, bf16[8,512]{1,0:T(8,128)(2,1)}, f32[8,1,256]{2,1,0:T(1,128)}, f32[1,8]{1,0:T(1,128)}) custom-call(f32[8,256]{1,0:T(8,128)} %get-tuple-element.14.admitted_in, f32[8,256]{1,0:T(8,128)} %get-tuple-element.15.values_in, f32[8,128]{1,0:T(8,128)} %get-tuple-element.16.keep_in, f32[8,1,256,256]{3,2,1,0:T(8,128)} %memory.3, ...), custom_call_target="tpu_custom_call" | custom-call | tf_op jit(solution)/shard_map/update/pallas_call | solution.py:717

commit v5 on v4

--- a/solution.py
+++ b/solution.py
@@ -370,6 +370,7 @@
         dispatch(group * GROUP, (group + 1) * GROUP, disp_send, tp, disp_sems.at[group], False)
     rows[tp, 0] = disp_send[ep]
     disp_opposite[...] = pick_quarter(opposite)
+    dispatch(NEP - GROUP // 2, NEP, disp_opposite, opposite, disp_sems.at[GROUPS], True)
 
     neighbours = (1, NTP - 1)
 
@@ -394,7 +395,9 @@
                 device_id_type=MESH,
             ).start()
         if group == 0:
-            dispatch(0, NEP, disp_opposite, opposite, disp_sems.at[GROUPS], True)
+            dispatch(NEP // 2, NEP - GROUP // 2, disp_opposite, opposite, disp_sems.at[GROUPS], True)
+        if group == 1:
+            dispatch(0, NEP // 2, disp_opposite, opposite, disp_sems.at[GROUPS], True)
             rows[opposite, 0] = disp_opposite[ep]
 
     for load in loads[6:]:

time: 43.3 us -> 43.2 us (level)
  no operation moved by 1% of the time
where the time goes in v5:
time: 43.2 us; the launch traced here: 43 us
  Pallas kernels  41.7 us (97%)
  between operations  1.29 us (3%)
    pallas_call x1, Pallas kernels, shards(): pl.pallas_call(kernel, out_shape=results, in_specs=[hbm] * 18 + [smem], o...  38.9 us
    pallas_call x1, Pallas kernels, shards(): pl.pallas_call(update_kernel, out_shape=(jax.ShapeDtypeStruct(memory.shap...  2.84 us

profile of v5, /device:TPU:1, one launch (start us, length us, event | category | flops | bytes accessed | tf_op | source)
XLA Modules:
  0.0 43.0 jit_solution(15416632414854550396)
XLA Ops:
  1.3 38.9 %layer.1 = (bf16[8,512]{1,0:T(8,128)(2,1)}, f32[8,256]{1,0:T(8,128)}, f32[8,256]{1,0:T(8,128)}, f32[8,128]{1,0:T(8,128)}, f32[8,1,256]{2,1,0:T(1,128)}, /*index=5*/f32[1,8]{1,0:T(1,128)}) custom-call(bf16[8,2048]{1,0:T(8,128)(2,1)} %tokens_in.1, f32[1,2048]{1,0:T(1,128)} %bitcast.12, f32[1,2048]{1,0:T(1,128)} %bitcast.13, bf16[1,2048]{1,0:T(2,128)(2,1)} %bitcast.14, ...), custom_call_target="tpu_custom_call" | custom-call | tf_op jit(solution)/shard_map/layer/pallas_call | solution.py:665
  40.2 2.8 %update.1 = (f32[8,1,256,256]{3,2,1,0:T(8,128)}, bf16[8,512]{1,0:T(8,128)(2,1)}, f32[8,1,256]{2,1,0:T(1,128)}, f32[1,8]{1,0:T(1,128)}) custom-call(f32[8,256]{1,0:T(8,128)} %get-tuple-element.14.admitted_in, f32[8,256]{1,0:T(8,128)} %get-tuple-element.15.values_in, f32[8,128]{1,0:T(8,128)} %get-tuple-element.16.keep_in, f32[8,1,256,256]{3,2,1,0:T(8,128)} %memory.3, ...), custom_call_target="tpu_custom_call" | custom-call | tf_op jit(solution)/shard_map/update/pallas_call | solution.py:720
